TPU v7x, 32 devices: a whole 2x2x4 slice. The times are simulated.
32 devices in a mesh: sp: 8 (over z, core), tp: 4 (over y, x).
Axes of the slice: x: 2, y: 2, z: 4, core: 2. Of those that a mesh axis runs over, the one named last changes fastest.
Arguments:
- cotangent: bfloat16 [1024, 2048], P('sp'), may hold values from -6 to 6
- moe_input: bfloat16 [1024, 2048], P('sp'), may hold values from -6 to 6
- expert_ids: int32 [1024, 2], P('sp'), may hold values from 0 to 7, all different within a row; in each aligned block of 128 rows (0 to 127, 128 to 255, ...) at most 48 rows name the same one
- group_weight: float32 [1024], P('sp'), may hold values from 0.3 to 1
- expert_weight: float32 [1024, 2], P('sp'), may hold values from 0.1 to 0.9
- mixer_out: bfloat16 [1024, 512], P('sp', 'tp'), may hold values from -6 to 6
- queries: bfloat16 [256, 1024], P('tp', 'sp'), may hold values from -6 to 6
- key_vectors: bfloat16 [256, 1024], P('tp', 'sp'), may hold values from -6 to 6
- value_vectors: bfloat16 [512, 1024], P('tp', 'sp'), may hold values from -6 to 6
- decay_rates: float32 [4, 1024], P('tp', 'sp'), may hold values from 0 to 1, as said below
- proj_weight: bfloat16 [2048, 512], P(None, 'tp'), may hold values from -0.25 to 0.25
- gate_weight: bfloat16 [8, 2048, 2048], P('sp', None, 'tp'), may hold values from -0.125 to 0.125
- up_weight: bfloat16 [8, 2048, 2048], P('sp', None, 'tp'), may hold values from -0.125 to 0.125
- down_weight: bfloat16 [8, 2048, 2048], P('sp', 'tp'), may hold values from -0.125 to 0.125
Outputs:
- grad_gate: bfloat16 [8, 2048, 2048], P('sp', None, 'tp')
- grad_up: bfloat16 [8, 2048, 2048], P('sp', None, 'tp')
- grad_down: bfloat16 [8, 2048, 2048], P('sp', 'tp')
- grad_proj: float32 [2048, 512], P('sp', 'tp')
- grad_queries: float32 [256, 1024], P('tp', 'sp')
- grad_keys: float32 [256, 1024], P('tp', 'sp')
- grad_values: float32 [512, 1024], P('tp', 'sp')
Inputs may be any that keep to these rules, and one draw needn't show every extreme that they name: `expert_ids`: in the rows of one device no expert is named by more than 48 entries, a bound that some block reaches; the 2 experts of a row differ. `decay_rates`: Positive.
All inputs are finite; a program needn't handle non-finite values.
Results may differ from a plain program's by a relative error of at most 0.0058.
Values may be sent and summed in bfloat16 or wider, within the bound.
A program may use at most 64 MiB of HBM per device.

v0:
```python
import functools

import jax
import jax.numpy as jnp
from jax import lax
from jax.experimental import pallas as pl
from jax.experimental.pallas import tpu as pltpu
from jax.sharding import PartitionSpec as P

MESH = pl.DeviceIdType.MESH
VMEM = pl.BlockSpec(memory_space=pltpu.VMEM)


def near_first(count):
    order = [0]
    for step in range(1, count // 2 + 1):
        order.append(step)
        if count - step != step:
            order.append(count - step)
    return order


def greet_all(sp_count, tp_count, sp_place, tp_place, along_tp):
    barrier = pltpu.get_barrier_semaphore()
    for k in range(1, sp_count):
        pl.semaphore_signal(
            barrier,
            inc=1,
            device_id={"sp": lax.rem(sp_place + k, sp_count), "tp": tp_place},
            device_id_type=MESH,
        )
    if along_tp:
        for m in range(1, tp_count):
            pl.semaphore_signal(
                barrier,
                inc=1,
                device_id={"sp": sp_place, "tp": lax.rem(tp_place + m, tp_count)},
                device_id_type=MESH,
            )


def greet_wait(sp_count, tp_count, along_tp):
    barrier = pltpu.get_barrier_semaphore()
    pl.semaphore_wait(barrier, sp_count - 1 + (tp_count - 1 if along_tp else 0))


def greet(sp_count, tp_count, sp_place, tp_place, along_tp):
    greet_all(sp_count, tp_count, sp_place, tp_place, along_tp)
    greet_wait(sp_count, tp_count, along_tp)


def remote(src, dst, send_sem, recv_sem, sp_place, tp_place):
    return pltpu.make_async_remote_copy(
        src_ref=src,
        dst_ref=dst,
        send_sem=send_sem,
        recv_sem=recv_sem,
        device_id={"sp": sp_place, "tp": tp_place},
        device_id_type=MESH,
    )


def state_side(here, there, count):
    return (here + count - there) // count


def dispatch_kernel(
    sp_count, tp_count, capacity, ids, group, weight, cot, inp, keys, values, rates,
    cot_full, inp_full, state_all, select, cot_src, inp_src, state, local_sem, send_one, recv_one, send_two, recv_two, send_state, recv_state,
):
    me = lax.axis_index("sp")
    q = lax.axis_index("tp")
    width = cot_src.shape[2]
    square = tp_count == 4
    order = near_first(sp_count)
    arrays = ((cot_src, cot_full), (inp_src, inp_full))

    def columns(full, block, place):
        return full.at[block, :, pl.ds(pl.multiple_of(place * width, width), width)]

    if square:
        across_x = (q // 2) * 2 + (1 - lax.rem(q, 2))
        across_y = (1 - q // 2) * 2 + lax.rem(q, 2)
        across_both = (1 - q // 2) * 2 + (1 - lax.rem(q, 2))
        peers = (across_x, across_y)
        origins = (across_x, across_y)
    else:
        peers = tuple(lax.rem(q + m, tp_count) for m in range(1, tp_count))
        origins = tuple(lax.rem(q + tp_count - m, tp_count) for m in range(1, tp_count))

    greet_all(sp_count, tp_count, me, q, True)
    tokens, top_count = ids.shape
    block_rows = cot_src.shape[1]
    experts_all = sp_count * block_rows // capacity
    mine = pl.ds(pl.multiple_of(q * width, width), width)
    expert = lax.broadcasted_iota(jnp.int32, (tokens, experts_all), 1)
    named = [(ids[:, j : j + 1] == expert).astype(jnp.float32) for j in range(top_count)]
    below = lax.broadcasted_iota(jnp.int32, (tokens, tokens), 0) > lax.broadcasted_iota(
        jnp.int32, (tokens, tokens), 1
    )
    before = jnp.dot(
        below.astype(jnp.float32).astype(jnp.bfloat16),
        sum(named).astype(jnp.bfloat16),
        preferred_element_type=jnp.float32,
    )
    slots = []
    scaled = []
    cot_mine = cot[:, mine].astype(jnp.float32)
    inp_mine = inp[:, mine]
    for j in range(top_count):
        rank = jnp.sum(named[j] * before, axis=1, keepdims=True).astype(jnp.int32)
        before = before + named[j]
        slots.append(ids[:, j : j + 1] * capacity + rank)
        scaled.append((cot_mine * (group[...] * weight[:, j : j + 1])).astype(jnp.bfloat16))
    slot = lax.broadcasted_iota(jnp.int32, (tokens, block_rows), 1)

    def rows_of(picked, values):
        return lax.dot_general(
            picked, values, (((0,), (0,)), ((), ())), preferred_element_type=jnp.float32
        )

    def pack(k):
        there = lax.rem(me + k, sp_count)
        picks = [
            (s == slot + there * block_rows).astype(jnp.float32).astype(jnp.bfloat16)
            for s in slots
        ]
        cot_src[there] = sum(rows_of(p, v) for p, v in zip(picks, scaled)).astype(jnp.bfloat16)
        either = sum(picks)
        inp_src[there] = rows_of(either, inp_mine).astype(jnp.bfloat16)
        select[there] = either
        return there

    waits = []
    own = []
    pack(0)
    pack(order[1])
    greet_wait(sp_count, tp_count, True)
    for a, (src, full) in enumerate(arrays):
        copy = pltpu.make_async_copy(src.at[me], columns(full, me, q), local_sem.at[a])
        copy.start()
        own.append(copy)
    for k in order[1:]:
        there = lax.rem(me + k, sp_count)
        if k != order[1]:
            pack(k)
        for a, (src, full) in enumerate(arrays):
            copy = remote(
                src.at[there], columns(full, me, q), send_one.at[a, k], recv_one.at[a, k], there, q
            )
            copy.start()
            waits.append(copy)
    exact = lax.Precision.HIGHEST
    heads, length = rates.shape
    key_size = keys.shape[0] // heads
    value_size = values.shape[0] // heads
    upto = lax.broadcasted_iota(jnp.int32, (length, length), 0) <= lax.broadcasted_iota(
        jnp.int32, (length, length), 1
    )
    for h in range(heads):
        rate = jnp.broadcast_to(rates[h : h + 1, :], (8, length))
        prefix = jnp.dot(
            rate, upto.astype(jnp.float32), precision=exact, preferred_element_type=jnp.float32
        )[0:1]
        ending = prefix[:, length - 1 : length]
        key = keys[h * key_size : (h + 1) * key_size, :].astype(jnp.float32)
        value = values[h * value_size : (h + 1) * value_size, :].astype(jnp.float32)
        first = h * (key_size + 8)
        for side, reach in enumerate((jnp.exp(prefix - ending), jnp.exp(-prefix))):
            state[side, first : first + key_size, :] = lax.dot_general(
                key * reach,
                value,
                (((1,), (1,)), ((), ())),
                precision=exact,
                preferred_element_type=jnp.float32,
            )
            state[side, first + key_size : first + key_size + 8, :] = jnp.broadcast_to(
                ending, (8, value_size)
            )
    own_state = pltpu.make_async_copy(state.at[0], state_all.at[me], local_sem.at[2])
    own_state.start()
    for k in order[1:]:
        there = lax.rem(me + k, sp_count)
        copy = remote(
            state.at[state_side(me, there, sp_count)],
            state_all.at[me],
            send_state.at[k],
            recv_state.at[k],
            there,
            q,
        )
        copy.start()
        waits.append(copy)

    def forward(k):
        block = lax.rem(me + sp_count - k, sp_count)
        for a, (src, full) in enumerate(arrays):
            if k == 0:
                own[a].wait()
            else:
                remote(
                    src.at[block], columns(full, block, q), send_one.at[a, k], recv_one.at[a, k], me, q
                ).wait_recv()
            for m, peer in enumerate(peers):
                piece = columns(full, block, q)
                copy = remote(piece, piece, send_two.at[a, k, m], recv_two.at[a, k, m], me, peer)
                copy.start()
                waits.append(copy)

    def arrived(a, k, m, place):
        block = lax.rem(me + sp_count - k, sp_count)
        piece = columns(arrays[a][1], block, place)
        remote(piece, piece, send_two.at[a, k, m], recv_two.at[a, k, m], me, q).wait_recv()
        return piece

    def relay(k):
        for a in range(2):
            for m, place in enumerate(origins):
                piece = arrived(a, k, m, place)
                if square and m == a:
                    copy = remote(
                        piece, piece, send_two.at[a, k, 2], recv_two.at[a, k, 2], me, peers[1 - a]
                    )
                    copy.start()
                    waits.append(copy)

    for number, k in enumerate(order):
        forward(k)
        if number:
            relay(order[number - 1])
    relay(order[-1])
    if square:
        for k in order:
            for a in range(2):
                arrived(a, k, 2, across_both)
    for k in order[1:]:
        source = lax.rem(me + sp_count - k, sp_count)
        remote(
            state.at[0], state_all.at[source], send_state.at[k], recv_state.at[k], me, q
        ).wait_recv()
    own_state.wait()
    for copy in waits:
        copy.wait_send()


def dispatch(ids, group, weight, cot, inp, keys, values, rates, capacity, rows, sp_count, tp_count):
    tokens, model_width = cot.shape
    width = model_width // tp_count
    heads = rates.shape[0]
    state_rows = keys.shape[0] + 8 * heads
    value_size = values.shape[0] // heads
    full = jax.ShapeDtypeStruct((sp_count, rows, model_width), cot.dtype)
    dma = pltpu.SemaphoreType.DMA
    return pl.pallas_call(
        functools.partial(dispatch_kernel, sp_count, tp_count, capacity),
        out_shape=(
            full,
            full,
            jax.ShapeDtypeStruct((sp_count, state_rows, value_size), jnp.float32),
            jax.ShapeDtypeStruct((sp_count, tokens, rows), jnp.bfloat16),
        ),
        in_specs=[VMEM] * 8,
        out_specs=(VMEM,) * 4,
        scratch_shapes=[
            pltpu.VMEM((sp_count, rows, width), cot.dtype),
            pltpu.VMEM((sp_count, rows, width), inp.dtype),
            pltpu.VMEM((2, state_rows, value_size), jnp.float32),
            dma((3,)),
            dma((2, sp_count)),
            dma((2, sp_count)),
            dma((2, sp_count, tp_count - 1)),
            dma((2, sp_count, tp_count - 1)),
            dma((sp_count,)),
            dma((sp_count,)),
        ],
        compiler_params=pltpu.CompilerParams(collective_id=0, has_side_effects=True),
    )(ids, group, weight, cot, inp, keys, values, rates)


def return_kernel(
    sp_count, tp_count, part, select, cot, resid,
    summed_in, outgoing, returned, send_rs, recv_rs, send_back, recv_back, send_ag, recv_ag,
):
    me = lax.axis_index("sp")
    q = lax.axis_index("tp")
    width = cot.shape[1] // tp_count
    order = near_first(sp_count)

    def columns(place):
        return pl.ds(pl.multiple_of(place * width, width), width)

    greet(sp_count, tp_count, me, q, True)
    waits = []
    far_first = order[::-1]
    for k in far_first:
        block = lax.rem(me + k, sp_count)
        for m in range(1, tp_count):
            peer = lax.rem(q + m, tp_count)
            copy = remote(
                part.at[block, :, columns(peer)],
                summed_in.at[m - 1, block],
                send_rs.at[k, m - 1],
                recv_rs.at[k, m - 1],
                me,
                peer,
            )
            copy.start()
            waits.append(copy)
    for k in far_first:
        block = lax.rem(me + k, sp_count)
        total = part[block, :, columns(q)].astype(jnp.float32)
        for m in range(1, tp_count):
            remote(
                part.at[block, :, columns(q)],
                summed_in.at[m - 1, block],
                send_rs.at[k, m - 1],
                recv_rs.at[k, m - 1],
                me,
                q,
            ).wait_recv()
            total = total + summed_in[m - 1, block].astype(jnp.float32)
        outgoing[block] = total.astype(outgoing.dtype)
        if k:
            copy = remote(
                outgoing.at[block], returned.at[me], send_back.at[k], recv_back.at[k], block, q
            )
            copy.start()
            waits.append(copy)
    total = jnp.dot(select[me], outgoing[me], preferred_element_type=jnp.float32)
    for k in far_first[:-1]:
        source = lax.rem(me + sp_count - k, sp_count)
        remote(
            outgoing.at[source], returned.at[source], send_back.at[k], recv_back.at[k], me, q
        ).wait_recv()
        total = total + jnp.dot(
            select[source], returned[source], preferred_element_type=jnp.float32
        )
    resid[:, columns(q)] = (cot[:, columns(q)].astype(jnp.float32) + total).astype(resid.dtype)
    for m in range(1, tp_count):
        piece = resid.at[:, columns(q)]
        copy = remote(
            piece, piece, send_ag.at[m - 1], recv_ag.at[m - 1], me, lax.rem(q + m, tp_count)
        )
        copy.start()
        waits.append(copy)
    for m in range(1, tp_count):
        piece = resid.at[:, columns(lax.rem(q + tp_count - m, tp_count))]
        remote(piece, piece, send_ag.at[m - 1], recv_ag.at[m - 1], me, q).wait_recv()
    for copy in waits:
        copy.wait_send()


def bring_back(part, select, cot, sp_count, tp_count):
    rows = part.shape[1]
    width = cot.shape[1] // tp_count
    dma = pltpu.SemaphoreType.DMA
    return pl.pallas_call(
        functools.partial(return_kernel, sp_count, tp_count),
        out_shape=jax.ShapeDtypeStruct(cot.shape, cot.dtype),
        in_specs=[VMEM] * 3,
        out_specs=VMEM,
        scratch_shapes=[
            pltpu.VMEM((tp_count - 1, sp_count, rows, width), part.dtype),
            pltpu.VMEM((sp_count, rows, width), part.dtype),
            pltpu.VMEM((sp_count, rows, width), part.dtype),
            dma((sp_count, tp_count - 1)),
            dma((sp_count, tp_count - 1)),
            dma((sp_count,)),
            dma((sp_count,)),
            dma((tp_count - 1,)),
            dma((tp_count - 1,)),
        ],
        compiler_params=pltpu.CompilerParams(collective_id=1, has_side_effects=True),
    )(part, select, cot)


def expert_forward(cot_blocks, inp_blocks, gate_weight, up_weight, down_weight):
    gate_pre = jnp.einsum(
        "secd,edf->secf", inp_blocks, gate_weight, preferred_element_type=jnp.float32
    )
    up_pre = jnp.einsum("secd,edf->secf", inp_blocks, up_weight, preferred_element_type=jnp.float32)
    sigmoid_gate = jax.nn.sigmoid(gate_pre)
    hidden = (gate_pre * sigmoid_gate * up_pre).astype(jnp.bfloat16)
    hidden_grad = jnp.einsum(
        "secd,efd->secf", cot_blocks, down_weight, preferred_element_type=jnp.float32
    )
    gate_grad = (
        hidden_grad * up_pre * sigmoid_gate * (1.0 + gate_pre * (1.0 - sigmoid_gate))
    ).astype(jnp.bfloat16)
    up_grad = (hidden_grad * gate_pre * sigmoid_gate).astype(jnp.bfloat16)
    partial_grad = jnp.einsum(
        "secf,edf->secd", gate_grad, gate_weight, preferred_element_type=jnp.float32
    )
    partial_grad = partial_grad + jnp.einsum(
        "secf,edf->secd", up_grad, up_weight, preferred_element_type=jnp.float32
    )
    return hidden, gate_grad, up_grad, partial_grad.astype(jnp.bfloat16)


def on_device(
    cotangent,
    moe_input,
    expert_ids,
    group_weight,
    expert_weight,
    mixer_out,
    queries,
    key_vectors,
    value_vectors,
    decay_rates,
    proj_weight,
    gate_weight,
    up_weight,
    down_weight,
):
    exact = lax.Precision.HIGHEST
    sp_count = lax.axis_size("sp")
    tp_count = lax.axis_size("tp")
    me = lax.axis_index("sp")
    local_experts = gate_weight.shape[0]
    experts_all = local_experts * sp_count
    rows_here, model_width = cotangent.shape
    top_count = expert_ids.shape[1]
    capacity = 3 * top_count * rows_here // (2 * experts_all)
    block_rows = local_experts * capacity

    heads_here, length = decay_rates.shape
    query_full = queries.astype(jnp.float32).reshape(heads_here, -1, length)
    key_full = key_vectors.astype(jnp.float32).reshape(heads_here, -1, length)
    value_full = value_vectors.astype(jnp.float32).reshape(heads_here, -1, length)
    key_size = query_full.shape[1]
    value_size = value_full.shape[1]
    score_scale = key_size ** (-0.5)
    place = jnp.arange(length, dtype=jnp.int32)
    prefix = jnp.dot(
        decay_rates, (place[:, None] <= place[None, :]).astype(jnp.float32), precision=exact
    )
    ending = prefix[:, -1:]
    mixing = score_scale * jnp.exp(-jnp.abs(prefix[:, :, None] - prefix[:, None, :]))
    toward_end = jnp.exp(prefix - ending)
    from_start = jnp.exp(-prefix)
    both_weights = jnp.stack([toward_end, from_start])
    got_cot, got_inp, key_states, select = dispatch(
        expert_ids,
        group_weight[:, None],
        expert_weight,
        cotangent,
        moe_input,
        key_vectors,
        value_vectors,
        decay_rates,
        capacity,
        block_rows,
        sp_count,
        tp_count,
    )
    key_states = key_states.reshape(sp_count, heads_here, -1, value_size)
    block_shape = (sp_count, local_experts, capacity, model_width)
    cot_blocks = got_cot.reshape(block_shape)
    inp_blocks = got_inp.reshape(block_shape)
    hidden, gate_grad, up_grad, partial_grad = expert_forward(
        cot_blocks, inp_blocks, gate_weight, up_weight, down_weight
    )

    resid_grad = bring_back(
        partial_grad.reshape(sp_count, block_rows, model_width), select, cotangent, sp_count, tp_count
    )
    grad_down = jnp.einsum(
        "secf,secd->efd", hidden, cot_blocks, preferred_element_type=jnp.float32
    ).astype(jnp.bfloat16)
    grad_gate = jnp.einsum(
        "secd,secf->edf", inp_blocks, gate_grad, preferred_element_type=jnp.float32
    ).astype(jnp.bfloat16)
    grad_up = jnp.einsum(
        "secd,secf->edf", inp_blocks, up_grad, preferred_element_type=jnp.float32
    ).astype(jnp.bfloat16)

    proj_part = lax.dot_general(
        resid_grad, mixer_out, (((0,), (0,)), ((), ())), preferred_element_type=jnp.float32
    ).astype(jnp.bfloat16)
    out_grad = lax.dot_general(
        proj_weight, resid_grad, (((0,), (1,)), ((), ())), preferred_element_type=jnp.float32
    ).reshape(heads_here, -1, length)
    query_state = jnp.einsum(
        "whkl,hvl->whkv", query_full[None] * both_weights[:, :, None, :], out_grad, precision=exact
    )
    block = jnp.arange(sp_count, dtype=jnp.int32)
    query_state = query_state.astype(jnp.bfloat16).transpose(0, 2, 1, 3)
    query_state = query_state.reshape(2, key_size, heads_here * value_size)
    sent = jnp.concatenate(
        [
            proj_part.reshape(sp_count, -1, heads_here * value_size),
            jnp.where((block > me)[:, None, None], query_state[:1], query_state[1:]),
        ],
        axis=1,
    )
    shared = lax.all_to_all(sent, "sp", split_axis=0, concat_axis=0, tiled=True)
    shared = shared.astype(jnp.float32)
    proj_rows = model_width // sp_count
    grad_proj = jnp.sum(shared[:, :proj_rows], axis=0)
    query_states = shared[:, proj_rows:].reshape(sp_count, key_size, heads_here, value_size)
    query_states = query_states.transpose(0, 2, 1, 3)

    totals = key_states[:, :, key_size, 0]
    low_between = (block[None, :] > block[:, None]) & (block[None, :] < me)
    high_between = (block[None, :] < block[:, None]) & (block[None, :] > me)
    low_decay = jnp.exp(-jnp.sum(jnp.where(low_between[:, :, None], totals[None], 0.0), axis=1))
    high_decay = jnp.exp(-jnp.sum(jnp.where(high_between[:, :, None], totals[None], 0.0), axis=1))
    low_decay = jnp.where((block < me)[:, None], low_decay, 0.0)
    high_decay = jnp.where((block > me)[:, None], high_decay, 0.0)
    both_decays = jnp.stack([low_decay, high_decay])[:, :, :, None, None]
    key_carried = jnp.sum(both_decays * key_states[None, :, :, :key_size], axis=1)
    query_carried = jnp.sum(both_decays * query_states[None], axis=1)

    scores = mixing * jnp.einsum("hkt,hks->hts", query_full, key_full, precision=exact)
    score_grad = mixing * jnp.einsum("hvt,hvs->hts", out_grad, value_full, precision=exact)
    query_grad = jnp.einsum("hks,hts->hkt", key_full, score_grad, precision=exact)
    key_grad = jnp.einsum("hkt,hts->hks", query_full, score_grad, precision=exact)
    value_grad = jnp.einsum("hvt,hts->hvs", out_grad, scores, precision=exact)
    reach = score_scale * jnp.stack([from_start, toward_end])
    out_reach = out_grad[None] * reach[:, :, None, :]
    value_reach = value_full[None] * reach[:, :, None, :]
    key_reach = key_full[None] * reach[:, :, None, :]
    query_grad = query_grad + jnp.einsum("whvl,whkv->hkl", out_reach, key_carried, precision=exact)
    key_grad = key_grad + jnp.einsum("whvl,whkv->hkl", value_reach, query_carried, precision=exact)
    value_grad = value_grad + jnp.einsum("whkl,whkv->hvl", key_reach, query_carried, precision=exact)
    return (
        grad_gate,
        grad_up,
        grad_down,
        grad_proj,
        query_grad.reshape(heads_here * key_size, length),
        key_grad.reshape(heads_here * key_size, length),
        value_grad.reshape(heads_here * value_size, length),
    )


def solution(mesh):
    return jax.shard_map(
        on_device,
        mesh=mesh,
        in_specs=(
            P("sp", None),
            P("sp", None),
            P("sp", None),
            P("sp"),
            P("sp", None),
            P("sp", "tp"),
            P("tp", "sp"),
            P("tp", "sp"),
            P("tp", "sp"),
            P("tp", "sp"),
            P(None, "tp"),
            P("sp", None, "tp"),
            P("sp", None, "tp"),
            P("sp", "tp", None),
        ),
        out_specs=(
            P("sp", None, "tp"),
            P("sp", None, "tp"),
            P("sp", "tp", None),
            P("sp", "tp"),
            P("tp", "sp"),
            P("tp", "sp"),
            P("tp", "sp"),
        ),
        check_vma=False,
    )
```

profile of v0, /device:TPU:0, one launch (start us, length us, event | category | flops | bytes accessed | tf_op | source)
XLA Modules:
  0.0 121.7 jit_solution(2256011318502300169)
XLA Ops:
  0.6 0.0 copy-start
  0.7 1.6 %copy.29.ids = s32[128,2]{1,0:T(8,128)} copy(s32[128,2]{0,1:T(2,128)} %param.16) | data formatting | bytes 2048 | tf_op args[2]
  2.2 1.4 %copy.30.group = f32[128,1]{1,0:T(8,128)} copy(f32[128,1]{0,1:T(1,128)} %bitcast.162) | data formatting | bytes 1024 | tf_op jit(solution)/shard_map/broadcast_in_dim | solution.py:445
  3.6 1.4 %copy.31.weight = f32[128,2]{1,0:T(8,128)} copy(f32[128,2]{0,1:T(2,128)} %param.18) | data formatting | bytes 2048 | tf_op args[4]
  5.0 0.8 fusion.38
  5.8 40.6 %shard_map.189 = (bf16[8,48,2048]{2,1,0:T(8,128)(2,1)}, bf16[8,48,2048]{2,1,0:T(8,128)(2,1)}, f32[8,72,128]{2,1,0:T(8,128)}, bf16[8,128,48]{2,1,0:T(8,128)(2,1)}) custom-call(s32[128,2]{1,0:T(8,128)} %copy.29.ids, f32[128,1]{1,0:T(8,128)} %copy.30.group, f32[128,2]{1,0:T(8,128)} %copy.31.weight, bf16[128,2048]{1,0:T(8,128)(2,1)} %cot.3, ...), custom_call_target="tpu_custom_call" | custom-call | tf_op jit(solution)/shard_map/pallas_call | solution.py:254
  46.5 3.1 %fusion.15 = f32[8,1,48,512]{3,2,0,1:T(8,128)S(1)} fusion(bf16[8,48,2048]{2,1,0:T(8,128)(2,1)} %get-tuple-element.11, bf16[1,2048,512]{2,1,0:T(8,128)(2,1)} %param.26), kind=kOutput, calls=%fused_computation.18 | convolution fusion | flops 805306368 | bytes 4456448 | tf_op jit(solution)/shard_map/secd,edf->secf/dot_general | solution.py:381
  49.6 0.0 copy-start.15
  49.7 1.0 fusion.18
  50.7 0.9 copy-done.15
  51.5 0.7 copy-done.16
  52.3 1.2 %multiply_convert_fusion.1 = (bf16[8,1,48,512]{3,2,0,1:T(8,128)(2,1)S(1)}, bf16[8,1,48,512]{3,2,0,1:T(8,128)(2,1)S(1)}) fusion(f32[8,1,48,512]{3,2,0,1:T(8,128)S(1)} %fusion.18, f32[8,1,48,512]{3,2,0,1:T(8,128)S(1)} %fusion.15, bf16[8,48,2048]{2,1,0:T(8,128)(2,1)S(1)} %copy-done.16, bf16[1,512,2048]{2,1,0:T(8,128)(2,1)S(1)} %copy-done.15), kind=kOutput, calls=%fused_computation.34 | convolution fusion | flops 807862272 | bytes 6029312 | tf_op jit(solution)/shard_map/secd,efd->secf/dot_general | solution.py:384
  53.5 0.0 copy-start.8
  53.5 0.0 copy-start.1
  53.5 1.0 fusion.3
  54.6 0.6 slice.23
  55.1 1.2 fusion.46
  56.3 2.2 %add_convert_fusion.part = bf16[8,48,2048]{2,1,0:T(8,128)(2,1)} fusion(f32[8,48,2048]{2,1,0:T(8,128)S(1)} %fusion.3, bf16[1,2048,512]{2,1,0:T(8,128)(2,1)S(1)} %copy-done.1, bf16[8,1,48,512]{3,2,0,1:T(8,128)(2,1)S(1)} %get-tuple-element.19), kind=kOutput, calls=%fused_computation.3 | convolution fusion | flops 806879232 | bytes 7208960 | tf_op jit(solution)/shard_map/secf,edf->secd/dot_general | solution.py:394
  58.5 31.1 %shard_map.190 = bf16[128,2048]{1,0:T(8,128)(2,1)} custom-call(bf16[8,48,2048]{2,1,0:T(8,128)(2,1)} %add_convert_fusion.part, bf16[8,128,48]{2,1,0:T(8,128)(2,1)} %get-tuple-element.13.select, bf16[128,2048]{1,0:T(8,128)(2,1)} %cot.3), custom_call_target="tpu_custom_call" | custom-call | tf_op jit(solution)/shard_map/pallas_call | solution.py:357
  89.7 1.3 %fusion.51 = f32[128,128]{1,0:T(8,128)S(1)} fusion(bf16[128,2048]{1,0:T(8,128)(2,1)} %shard_map.190, bf16[2048,128]{1,0:T(8,128)(2,1)S(1)} %copy-done.2), kind=kOutput, calls=%fused_computation.87 | convolution fusion | flops 67108864 | bytes 1114112 | tf_op jit(solution)/shard_map/dot_general | solution.py:481
  91.0 0.2 fusion.21
  91.3 0.0 copy-start.4
  91.3 1.4 %convolution_convert_fusion = bf16[2048,128]{1,0:T(8,128)(2,1)S(1)} fusion(bf16[128,2048]{1,0:T(8,128)(2,1)} %shard_map.190, bf16[128,128]{1,0:T(8,128)(2,1)S(1)} %copy-done.10), kind=kOutput, calls=%fused_computation.7 | convolution fusion | flops 67371008 | bytes 1081344 | tf_op jit(solution)/shard_map/dot_general | solution.py:478
  92.7 0.1 broadcast_select_fusion
  92.8 0.9 pad_maximum_fusion
  93.7 3.8 %all-to-all-start = ((bf16[8,320,128]{2,1,0:T(8,128)(2,1)}), bf16[8,320,128]{2,1,0:T(8,128)(2,1)S(1)}, u32[]{:S(2)}, u32[]{:S(2)}) async-start(bf16[8,320,128]{2,1,0:T(8,128)(2,1)} %pad_maximum_fusion), calls=%async_computation | async-start | bytes 1310720 | tf_op jit(solution)/shard_map/all_to_all | solution.py:497
  97.4 0.5 iota_compare_fusion.4
  98.0 1.4 %slice_reduce_fusion.1 = f32[8]{0:T(128)} fusion(f32[8,1,72,128]{3,2,0,1:T(8,128)} %bitcast.156), kind=kLoop, calls=%fused_computation.65 | loop fusion | bytes 64 | tf_op jit(solution)/shard_map/slice | solution.py:504
  99.4 1.0 slice_bitcast_fusion
  100.4 1.6 %convolution_multiply_fusion = f32[128,128]{1,0:T(8,128)} fusion(bf16[64,128]{1,0:T(8,128)(2,1)} %param.20, bf16[64,128]{1,0:T(8,128)(2,1)S(1)} %copy-done.6, f32[128]{0:T(128)} %bitcast.158), kind=kOutput, calls=%fused_computation.22 | convolution fusion | flops 2179072 | bytes 98816 | tf_op jit(solution)/shard_map/hkt,hks->hts/dot_general | solution.py:515
  101.9 0.9 convolution_multiply_fusion.1
  102.8 0.6 convert_element_type.74
  103.5 1.5 %convolution_bitcast_fusion.2 = f32[64,128]{1,0:T(8,128)} fusion(f32[128,128]{1,0:T(8,128)S(1)} %convolution_multiply_fusion.1, bf16[64,128]{1,0:T(8,128)(2,1)} %param.20), kind=kOutput, calls=%fused_computation.28 | convolution fusion | flops 12582912 | bytes 114688 | tf_op jit(solution)/shard_map/hkt,hts->hks/dot_general | solution.py:518
  105.0 0.2 convolution_bitcast_fusion.4
  105.1 0.0 copy-start.13
  105.2 4.0 %fusion.1 = bf16[1,2048,512]{2,1,0:T(8,128)(2,1)} fusion(bf16[8,48,2048]{2,1,0:T(8,128)(2,1)} %get-tuple-element.11, bf16[8,1,48,512]{3,2,0,1:T(8,128)(2,1)S(1)} %get-tuple-element.19), kind=kOutput, calls=%fused_computation.5 | convolution fusion | flops 806354944 | bytes 4063232 | tf_op jit(solution)/shard_map/secd,secf->edf/dot_general | solution.py:474
  109.2 0.1 copy.32
  109.3 0.8 select_reduce_fusion.1
  110.2 0.7 maximum_multiply_fusion
  110.9 4.2 %fusion = bf16[1,2048,512]{2,1,0:T(8,128)(2,1)} fusion(bf16[8,48,2048]{2,1,0:T(8,128)(2,1)} %get-tuple-element.11, bf16[8,1,48,512]{3,2,0,1:T(8,128)(2,1)} %copy-done.3), kind=kOutput, calls=%fused_computation.4 | convolution fusion | flops 806354944 | bytes 4063232 | tf_op jit(solution)/shard_map/secd,secf->edf/dot_general | solution.py:471
  115.1 2.7 %fusion.2 = bf16[1,512,2048]{2,1,0:T(8,128)(2,1)} fusion(bf16[8,48,2048]{2,1,0:T(8,128)(2,1)S(1)} %copy-done.17, f32[8,1,48,512]{3,2,0,1:T(8,128)S(1)} %copy-done.20, f32[8,1,48,512]{3,2,0,1:T(8,128)S(1)} %copy-done.22), kind=kOutput, calls=%fused_computation.6 | convolution fusion | flops 807534592 | bytes 5242880 | tf_op jit(solution)/shard_map/secf,secd->efd/dot_general | solution.py:468
  117.8 0.1 convert_element_type.73
  117.9 0.7 slice_reduce_fusion
  118.6 0.1 multiply_reduce_fusion
  118.8 0.3 convolution_bitcast_fusion
  119.1 0.9 convolution_add_fusion
  120.0 0.8 fusion.22
  120.8 0.8 fusion.23
  (47 shorter events, 0.1 us)
Async XLA Ops:
  0.6 49.0 %copy-start = (bf16[1,2048,512]{2,1,0:T(8,128)(2,1)S(1)}, bf16[1,2048,512]{2,1,0:T(8,128)(2,1)}, u32[]{:S(2)}) copy-start(bf16[1,2048,512]{2,1,0:T(8,128)(2,1)} %param.25) | copy-start | bytes 6291460
  5.8 49.3 %copy-start.11 = (f32[1,128]{1,0:T(1,128)}, f32[1,128]{1,0:T(1,128)S(1)}, u32[]{:S(2)}) copy-start(f32[1,128]{1,0:T(1,128)S(1)} %fusion.38) | copy-start | bytes 1540
  46.4 3.2 %copy-start.18 = (bf16[8,48,2048]{2,1,0:T(8,128)(2,1)S(1)}, bf16[8,48,2048]{2,1,0:T(8,128)(2,1)}, u32[]{:S(2)}) copy-start(bf16[8,48,2048]{2,1,0:T(8,128)(2,1)} %get-tuple-element.11) | copy-start | bytes 4718596
  49.6 1.0 copy-start.19
  49.6 1.9 %copy-start.15 = (bf16[1,512,2048]{2,1,0:T(8,128)(2,1)S(1)}, bf16[1,512,2048]{2,1,0:T(8,128)(2,1)}, u32[]{:S(2)}) copy-start(bf16[1,512,2048]{2,1,0:T(8,128)(2,1)} %param.27) | copy-start | bytes 6291460
  49.7 2.6 %copy-start.16 = (bf16[8,48,2048]{2,1,0:T(8,128)(2,1)S(1)}, bf16[8,48,2048]{2,1,0:T(8,128)(2,1)}, u32[]{:S(2)}) copy-start(bf16[8,48,2048]{2,1,0:T(8,128)(2,1)} %get-tuple-element.12) | copy-start | bytes 4718596
  50.6 2.8 %copy-start.21 = (f32[8,1,48,512]{3,2,0,1:T(8,128)}, f32[8,1,48,512]{3,2,0,1:T(8,128)S(1)}, u32[]{:S(2)}) copy-start(f32[8,1,48,512]{3,2,0,1:T(8,128)S(1)} %fusion.18) | copy-start | bytes 2359300
  53.5 1.0 copy-start.3
  53.5 2.8 %copy-start.8 = (bf16[64,128]{1,0:T(8,128)(2,1)S(1)}, bf16[64,128]{1,0:T(8,128)(2,1)}, u32[]{:S(2)}) copy-start(bf16[64,128]{1,0:T(8,128)(2,1)} %param.20) | copy-start | bytes 49156
  53.5 2.8 %copy-start.1 = (bf16[1,2048,512]{2,1,0:T(8,128)(2,1)S(1)}, bf16[1,2048,512]{2,1,0:T(8,128)(2,1)}, u32[]{:S(2)}) copy-start(bf16[1,2048,512]{2,1,0:T(8,128)(2,1)} %param.26) | copy-start | bytes 6291460
  58.5 31.1 %copy-start.2 = (bf16[2048,128]{1,0:T(8,128)(2,1)S(1)}, bf16[2048,128]{1,0:T(8,128)(2,1)}, u32[]{:S(2)}) copy-start(bf16[2048,128]{1,0:T(8,128)(2,1)} %param.24) | copy-start | bytes 1572868
  58.5 32.7 %copy-start.10 = (bf16[128,128]{1,0:T(8,128)(2,1)S(1)}, bf16[128,128]{1,0:T(8,128)(2,1)}, u32[]{:S(2)}) copy-start(bf16[128,128]{1,0:T(8,128)(2,1)} %param.19) | copy-start | bytes 98308
  91.3 6.7 %copy-start.12 = (pred[8]{0:T(512)(128)(4,1)}, pred[8]{0:T(512)(128)(4,1)S(1)}, u32[]{:S(2)}) copy-start(pred[8]{0:T(512)(128)(4,1)S(1)} %iota_compare_fusion.5) | copy-start | bytes 28
  91.3 9.1 %copy-start.6 = (bf16[64,128]{1,0:T(8,128)(2,1)S(1)}, bf16[64,128]{1,0:T(8,128)(2,1)}, u32[]{:S(2)}) copy-start(bf16[64,128]{1,0:T(8,128)(2,1)} %keys.1) | copy-start | bytes 49156
  91.3 10.6 %copy-start.4 = (bf16[128,128]{1,0:T(8,128)(2,1)S(1)}, bf16[128,128]{1,0:T(8,128)(2,1)}, u32[]{:S(2)}) copy-start(bf16[128,128]{1,0:T(8,128)(2,1)} %values.1) | copy-start | bytes 98308
  93.7 24.1 %all-to-all-start = ((bf16[8,320,128]{2,1,0:T(8,128)(2,1)}), bf16[8,320,128]{2,1,0:T(8,128)(2,1)S(1)}, u32[]{:S(2)}, u32[]{:S(2)}) async-start(bf16[8,320,128]{2,1,0:T(8,128)(2,1)} %pad_maximum_fusion), calls=%async_computation | async-start | bytes 1310720 | tf_op jit(solution)/shard_map/all_to_all | solution.py:497
  105.1 4.2 %copy-start.13 = (pred[8]{0:T(512)(128)(4,1)S(1)}, pred[8]{0:T(512)(128)(4,1)}, u32[]{:S(2)}) copy-start(pred[8]{0:T(512)(128)(4,1)} %copy-done.12) | copy-start | bytes 28
  105.2 4.1 %copy-start.14 = (f32[8]{0:T(128)S(1)}, f32[8]{0:T(128)}, u32[]{:S(2)}) copy-start(f32[8]{0:T(128)} %slice_reduce_fusion.1) | copy-start | bytes 100
  110.8 4.3 %copy-start.17 = (bf16[8,48,2048]{2,1,0:T(8,128)(2,1)S(1)}, bf16[8,48,2048]{2,1,0:T(8,128)(2,1)}, u32[]{:S(2)}) copy-start(bf16[8,48,2048]{2,1,0:T(8,128)(2,1)} %get-tuple-element.12) | copy-start | bytes 4718596
  110.8 4.3 %copy-start.20 = (f32[8,1,48,512]{3,2,0,1:T(8,128)S(1)}, f32[8,1,48,512]{3,2,0,1:T(8,128)}, u32[]{:S(2)}) copy-start(f32[8,1,48,512]{3,2,0,1:T(8,128)} %copy-done.19) | copy-start | bytes 2359300
  110.9 4.3 %copy-start.22 = (f32[8,1,48,512]{3,2,0,1:T(8,128)S(1)}, f32[8,1,48,512]{3,2,0,1:T(8,128)}, u32[]{:S(2)}) copy-start(f32[8,1,48,512]{3,2,0,1:T(8,128)} %copy-done.21) | copy-start | bytes 2359300
  117.8 1.3 %copy-start.9 = (f32[128,128]{1,0:T(8,128)S(1)}, f32[128,128]{1,0:T(8,128)}, u32[]{:S(2)}) copy-start(f32[128,128]{1,0:T(8,128)} %convolution_multiply_fusion) | copy-start | bytes 196612
  117.8 2.2 %copy-start.5 = (f32[128,128]{1,0:T(8,128)S(1)}, f32[128,128]{1,0:T(8,128)}, u32[]{:S(2)}) copy-start(f32[128,128]{1,0:T(8,128)} %convert_element_type.74) | copy-start | bytes 196612
  117.8 2.2 %copy-start.7 = (f32[64,128]{1,0:T(8,128)S(1)}, f32[64,128]{1,0:T(8,128)}, u32[]{:S(2)}) copy-start(f32[64,128]{1,0:T(8,128)} %convolution_bitcast_fusion.2) | copy-start | bytes 98308
where the time goes:
time: 122 us
  Pallas kernels  71.7 us (59%)
  matrix products  30.2 us (25%)
  local copies, waits for them, and re-layouts  9.15 us (8%)
  other arithmetic  5.75 us (5%)
  starting transfers between devices  3.78 us (3%)
    pallas_call x1, Pallas kernels, dispatch(): pl.pallas_call(functools.partial(dispatch_kernel, sp_count, tp_count, cap...  40.6 us
    pallas_call x1, Pallas kernels, bring_back(): pl.pallas_call(functools.partial(return_kernel, sp_count, tp_count), out_...  31.1 us
    unnamed x48, local copies, waits for them, and re-layouts  4.69 us
    dot_general x1, matrix products, on_device(): jnp.einsum('secd,secf->edf', inp_blocks, gate_grad, preferred_element_typ...  4.24 us
    dot_general x1, matrix products, on_device(): jnp.einsum('secd,secf->edf', inp_blocks, up_grad, preferred_element_type=...  4.02 us
    all_to_all x1, starting transfers between devices, on_device(): shared = lax.all_to_all(sent, 'sp', split_axis=0, concat_axis=0, tiled=True)  3.78 us
    dot_general x1, matrix products, expert_forward(): jnp.einsum('secd,edf->secf', inp_blocks, up_weight, preferred_element_typ...  3.15 us
    dot_general x1, matrix products, on_device(): jnp.einsum('secf,secd->efd', hidden, cot_blocks, preferred_element_type=j...  2.67 us
  transfers between devices with their start and end apart: 1, of which 0 were waited for; matrix products, arithmetic and copies ran while one was open for 17% of the time, Pallas kernels for 0%

commit v1 on v0

v1 whole, which is shorter than its diff:
```python
import functools

import jax
import jax.numpy as jnp
from jax import lax
from jax.experimental import pallas as pl
from jax.experimental.pallas import tpu as pltpu
from jax.sharding import PartitionSpec as P

MESH = pl.DeviceIdType.MESH
VMEM = pl.BlockSpec(memory_space=pltpu.VMEM)
ANY = pl.BlockSpec(memory_space=pl.ANY)


def partner(place, k, count):
    if k == 0:
        return place
    out = 0
    bit = 1
    while bit < count:
        b = lax.rem(place // bit, 2)
        out = out + bit * ((1 - b) if k & bit else b)
        bit *= 2
    return out


def remote(src, dst, send_sem, recv_sem, sp_place, tp_place):
    return pltpu.make_async_remote_copy(
        src_ref=src,
        dst_ref=dst,
        send_sem=send_sem,
        recv_sem=recv_sem,
        device_id={"sp": sp_place, "tp": tp_place},
        device_id_type=MESH,
    )


def state_side(here, there, count):
    return (here + count - there) // count


def dot(a, b, a_dim, b_dim):
    return lax.dot_general(
        a, b, (((a_dim,), (b_dim,)), ((), ())), preferred_element_type=jnp.float32
    )


def experts_kernel(
    sp_count, tp_count, groups,
    ids, group, weight, rates, keys, values, cot_hbm, inp_hbm, gate_hbm, up_hbm, down_hbm,
    resid, state_all, grad_gate, grad_up, grad_down,
    cot, inp, w_gate, w_up, w_down, picks, either, scaled, z_src, pair_src, rows, state,
    hidden, gate_grad, up_grad, part, own_part, summed_in, outgoing, returned,
    load_sem, send_z, recv_z, send_xy, recv_xy, send_far, recv_far, send_state, recv_state,
    send_rs, recv_rs, send_back, recv_back, send_ag, recv_ag,
):
    me = lax.axis_index("sp")
    q = lax.axis_index("tp")
    tokens, model_width = cot.shape
    width = model_width // tp_count
    block_rows = rows.shape[2]
    hidden_width = w_gate.shape[1]
    square = tp_count == 4
    at = [partner(me, k, sp_count) for k in range(sp_count)]
    peer = [partner(q, m, tp_count) for m in range(tp_count)]

    def columns(place):
        return pl.ds(pl.multiple_of(place * width, width), width)

    mine = columns(q)
    loads = []
    for i, (src, dst) in enumerate(
        (
            (cot_hbm, cot),
            (inp_hbm, inp),
            (gate_hbm.at[0], w_gate),
            (up_hbm.at[0], w_up),
            (down_hbm.at[0], w_down),
        )
    ):
        copy = pltpu.make_async_copy(src, dst, load_sem.at[i])
        copy.start()
        loads.append(copy)

    barrier = pltpu.get_barrier_semaphore()
    for k in range(1, sp_count):
        pl.semaphore_signal(
            barrier, inc=1, device_id={"sp": at[k], "tp": q}, device_id_type=MESH
        )
    for m in range(1, tp_count):
        pl.semaphore_signal(
            barrier, inc=1, device_id={"sp": me, "tp": peer[m]}, device_id_type=MESH
        )

    top_count = ids.shape[0]
    expert = lax.broadcasted_iota(jnp.int32, (sp_count, tokens), 0)
    named = [(ids[j : j + 1, :] == expert).astype(jnp.float32) for j in range(top_count)]
    earlier = lax.broadcasted_iota(jnp.int32, (tokens, tokens), 0) < lax.broadcasted_iota(
        jnp.int32, (tokens, tokens), 1
    )
    before = jnp.dot(
        sum(named).astype(jnp.bfloat16),
        earlier.astype(jnp.float32).astype(jnp.bfloat16),
        preferred_element_type=jnp.float32,
    )
    slots = []
    route = jnp.zeros((8, tokens), jnp.float32)
    lane_of = lax.broadcasted_iota(jnp.int32, (8, tokens), 0)
    for j in range(top_count):
        rank = jnp.sum(named[j] * before, axis=0, keepdims=True).astype(jnp.int32)
        before = before + named[j]
        slots.append(ids[j : j + 1, :] * block_rows + rank)
        route = jnp.where(lane_of == j, group[...] * weight[j : j + 1, :], route)
    route = jnp.transpose(route)
    row_of = lax.broadcasted_iota(jnp.int32, (block_rows, tokens), 0)
    for k in range(sp_count):
        here = pl.ds(k * block_rows, block_rows)
        pick = [(s == row_of + at[k] * block_rows).astype(jnp.float32) for s in slots]
        for j in range(top_count):
            picks[here, j * tokens : (j + 1) * tokens] = pick[j].astype(jnp.bfloat16)
        either[here, :] = sum(pick).astype(jnp.bfloat16)

    loads[0].wait()
    loads[1].wait()
    cot_mine = cot[:, mine].astype(jnp.float32)
    scaled_mine = jnp.concatenate(
        [(cot_mine * route[:, j : j + 1]).astype(jnp.bfloat16) for j in range(top_count)], axis=0
    )
    first = 2 * block_rows
    cot_out = jnp.dot(picks[first:, :], scaled_mine, preferred_element_type=jnp.float32)
    inp_out = jnp.dot(either[first:, :], inp[:, mine], preferred_element_type=jnp.float32)
    for k in range(2, sp_count):
        here = slice((k - 2) * block_rows, (k - 1) * block_rows)
        z_src[k, 0] = cot_out[here].astype(z_src.dtype)
        z_src[k, 1] = inp_out[here].astype(z_src.dtype)
    pl.semaphore_wait(barrier, sp_count - 1 + tp_count - 1)

    waits = []

    def send(copy):
        copy.start()
        waits.append(copy)

    for k in range(2, sp_count):
        send(remote(z_src.at[k], rows.at[:, k, :, mine], send_z.at[k], recv_z.at[k], at[k], q))

    cot_all = cot[...].astype(jnp.float32)
    for j in range(top_count):
        scaled[j * tokens : (j + 1) * tokens, :] = (cot_all * route[:, j : j + 1]).astype(scaled.dtype)
    cot_out = jnp.dot(picks[:first, :], scaled[...], preferred_element_type=jnp.float32)
    inp_out = jnp.dot(either[:first, :], inp[...], preferred_element_type=jnp.float32)
    pair_src[0] = cot_out[block_rows:].astype(pair_src.dtype)
    pair_src[1] = inp_out[block_rows:].astype(pair_src.dtype)
    send(remote(pair_src, rows.at[:, 1], send_z.at[1], recv_z.at[1], at[1], q))
    rows[0, 0] = cot_out[:block_rows].astype(rows.dtype)
    rows[1, 0] = inp_out[:block_rows].astype(rows.dtype)

    exact = lax.Precision.HIGHEST
    heads, length = rates.shape
    key_size = keys.shape[0] // heads
    value_size = values.shape[0] // heads
    upto = lax.broadcasted_iota(jnp.int32, (length, length), 0) <= lax.broadcasted_iota(
        jnp.int32, (length, length), 1
    )
    for h in range(heads):
        rate = jnp.broadcast_to(rates[h : h + 1, :], (8, length))
        prefix = jnp.dot(
            rate, upto.astype(jnp.float32), precision=exact, preferred_element_type=jnp.float32
        )[0:1]
        ending = prefix[:, length - 1 : length]
        key = keys[h * key_size : (h + 1) * key_size, :].astype(jnp.float32)
        value = values[h * value_size : (h + 1) * value_size, :].astype(jnp.float32)
        top = h * (key_size + 8)
        for side, reach in enumerate((jnp.exp(prefix - ending), jnp.exp(-prefix))):
            state[side, top : top + key_size, :] = lax.dot_general(
                key * reach,
                value,
                (((1,), (1,)), ((), ())),
                precision=exact,
                preferred_element_type=jnp.float32,
            )
            state[side, top + key_size : top + key_size + 8, :] = jnp.broadcast_to(
                ending, (8, value_size)
            )
    state_all[me] = state[0]
    for k in range(1, sp_count):
        send(
            remote(
                state.at[state_side(me, at[k], sp_count)],
                state_all.at[me],
                send_state.at[k],
                recv_state.at[k],
                at[k],
                q,
            )
        )

    def land(g):
        for k in range(*groups[g]):
            if k < 2:
                continue
            piece = rows.at[:, k, :, mine]
            remote(z_src.at[k], piece, send_z.at[k], recv_z.at[k], me, q).wait_recv()
            for m in range(1, tp_count):
                if square and m == 3:
                    continue
                send(
                    remote(piece, piece, send_xy.at[k, m - 1], recv_xy.at[k, m - 1], me, peer[m])
                )

    def relay(g):
        for k in range(*groups[g]):
            if k < 2:
                continue
            for m in range(1, tp_count):
                if square and m == 3:
                    continue
                piece = rows.at[:, k, :, columns(peer[m])]
                remote(piece, piece, send_xy.at[k, m - 1], recv_xy.at[k, m - 1], me, q).wait_recv()
                if square:
                    a = m - 1
                    half = rows.at[a, k, :, columns(peer[m])]
                    send(
                        remote(half, half, send_far.at[a, k], recv_far.at[a, k], me, peer[3 - m])
                    )

    def settle(g):
        for k in range(*groups[g]):
            if k == 1:
                remote(pair_src, rows.at[:, 1], send_z.at[1], recv_z.at[1], me, q).wait_recv()
            if k >= 2 and square:
                for a in range(2):
                    piece = rows.at[a, k, :, columns(peer[3])]
                    remote(piece, piece, send_far.at[a, k], recv_far.at[a, k], me, q).wait_recv()

    def forward(g):
        low, high = groups[g]
        count = high - low
        size = count * block_rows
        here = slice(low * block_rows, high * block_rows)
        got = rows[1, low:high].reshape(size, model_width)
        gate_pre = jnp.dot(got, w_gate[...], preferred_element_type=jnp.float32)
        up_pre = jnp.dot(got, w_up[...], preferred_element_type=jnp.float32)
        sigmoid_gate = jax.nn.sigmoid(gate_pre)
        silu_gate = gate_pre * sigmoid_gate
        hidden[here, :] = (silu_gate * up_pre).astype(hidden.dtype)
        got = rows[0, low:high].reshape(size, model_width)
        hidden_grad = dot(got, w_down[...], 1, 1)
        gate_rows = (
            hidden_grad * up_pre * sigmoid_gate * (1.0 + gate_pre * (1.0 - sigmoid_gate))
        ).astype(jnp.bfloat16)
        up_rows = (hidden_grad * silu_gate).astype(jnp.bfloat16)
        gate_grad[here, :] = gate_rows
        up_grad[here, :] = up_rows
        for m in list(range(tp_count - 1, 0, -1)) + [0]:
            theirs = columns(peer[m])
            partial = dot(gate_rows, w_gate[theirs, :], 1, 1) + dot(up_rows, w_up[theirs, :], 1, 1)
            partial = partial.reshape(count, block_rows, width)
            if m == 0:
                own_part[low:high] = partial
            else:
                part[m - 1, low:high] = partial.astype(part.dtype)
                send(
                    remote(
                        part.at[m - 1, pl.ds(low, count)],
                        summed_in.at[m - 1, pl.ds(low, count)],
                        send_rs.at[g, m - 1],
                        recv_rs.at[g, m - 1],
                        me,
                        peer[m],
                    )
                )

    def give_back(g):
        low, high = groups[g]
        count = high - low
        total = own_part[low:high]
        for m in range(1, tp_count):
            piece = summed_in.at[m - 1, pl.ds(low, count)]
            remote(piece, piece, send_rs.at[g, m - 1], recv_rs.at[g, m - 1], me, q).wait_recv()
            total = total + summed_in[m - 1, low:high].astype(jnp.float32)
        total = total.astype(outgoing.dtype)
        for k in range(low, high):
            if k == 0:
                returned[0] = total[0]
            else:
                outgoing[k] = total[k - low]
                send(
                    remote(
                        outgoing.at[k], returned.at[k], send_back.at[k], recv_back.at[k], at[k], q
                    )
                )

    all_rows = sp_count * block_rows

    def down_grads():
        got = rows[0].reshape(all_rows, model_width)
        for m in range(tp_count):
            cut = slice(m * width, (m + 1) * width)
            grad_down[:, cut] = dot(hidden[...], got[:, cut], 0, 0).astype(grad_down.dtype)

    def input_grads(grads, out):
        for m in range(tp_count):
            cut = slice(m * width, (m + 1) * width)
            got = rows[1, :, :, cut].reshape(all_rows, width)
            out[cut, :] = dot(got, grads[...], 0, 0).astype(out.dtype)

    count = len(groups)
    land(0)
    land(1)
    relay(0)
    for load in loads[2:]:
        load.wait()
    settle(0)
    forward(0)
    for g in range(1, count):
        relay(g)
        if g + 1 < count:
            land(g + 1)
        elif g >= 2:
            give_back(0)
        settle(g)
        forward(g)
    for g in range(0 if count <= 2 else 1, count - 1):
        give_back(g)
    down_grads()
    give_back(count - 1)
    input_grads(gate_grad, grad_gate)
    for k in range(1, sp_count):
        remote(
            outgoing.at[k], returned.at[k], send_back.at[k], recv_back.at[k], me, q
        ).wait_recv()
    total = dot(either[...], returned[...].reshape(all_rows, width), 0, 0)
    resid[:, mine] = (cot[:, mine].astype(jnp.float32) + total).astype(resid.dtype)
    piece = resid.at[:, mine]
    for m in range(tp_count - 1, 0, -1):
        send(remote(piece, piece, send_ag.at[m - 1], recv_ag.at[m - 1], me, peer[m]))
    input_grads(up_grad, grad_up)
    for m in range(1, tp_count):
        piece = resid.at[:, columns(peer[m])]
        remote(piece, piece, send_ag.at[m - 1], recv_ag.at[m - 1], me, q).wait_recv()
    for k in range(1, sp_count):
        piece = state_all.at[at[k]]
        remote(piece, piece, send_state.at[k], recv_state.at[k], me, q).wait_recv()
    for copy in waits:
        copy.wait_send()


def experts(
    ids, group, weight, rates, keys, values, cot, inp, gate, up, down, capacity, sp_count, tp_count
):
    tokens, model_width = cot.shape
    width = model_width // tp_count
    hidden_width = gate.shape[2]
    heads = rates.shape[0]
    state_rows = keys.shape[0] + 8 * heads
    value_size = values.shape[0] // heads
    block_rows = -(-capacity // 16) * 16
    all_rows = sp_count * block_rows
    quarter = sp_count // 4
    groups = [(i * quarter, (i + 1) * quarter) for i in range(4)]
    kind = cot.dtype
    dma = pltpu.SemaphoreType.DMA
    vmem = pltpu.VMEM
    return pl.pallas_call(
        functools.partial(experts_kernel, sp_count, tp_count, groups),
        out_shape=(
            jax.ShapeDtypeStruct((tokens, model_width), kind),
            jax.ShapeDtypeStruct((sp_count, state_rows, value_size), jnp.float32),
            jax.ShapeDtypeStruct((model_width, hidden_width), kind),
            jax.ShapeDtypeStruct((model_width, hidden_width), kind),
            jax.ShapeDtypeStruct((hidden_width, model_width), kind),
        ),
        in_specs=[VMEM] * 6 + [ANY] * 5,
        out_specs=(VMEM,) * 5,
        scratch_shapes=[
            vmem((tokens, model_width), kind),
            vmem((tokens, model_width), kind),
            vmem((model_width, hidden_width), kind),
            vmem((model_width, hidden_width), kind),
            vmem((hidden_width, model_width), kind),
            vmem((all_rows, ids.shape[0] * tokens), jnp.bfloat16),
            vmem((all_rows, tokens), jnp.bfloat16),
            vmem((ids.shape[0] * tokens, model_width), kind),
            vmem((sp_count, 2, block_rows, width), kind),
            vmem((2, block_rows, model_width), kind),
            vmem((2, sp_count, block_rows, model_width), kind),
            vmem((2, state_rows, value_size), jnp.float32),
            vmem((all_rows, hidden_width), kind),
            vmem((all_rows, hidden_width), kind),
            vmem((all_rows, hidden_width), kind),
            vmem((tp_count - 1, sp_count, block_rows, width), kind),
            vmem((sp_count, block_rows, width), jnp.float32),
            vmem((tp_count - 1, sp_count, block_rows, width), kind),
            vmem((sp_count, block_rows, width), kind),
            vmem((sp_count, block_rows, width), kind),
            dma((5,)),
            dma((sp_count,)),
            dma((sp_count,)),
            dma((sp_count, tp_count - 1)),
            dma((sp_count, tp_count - 1)),
            dma((2, sp_count)),
            dma((2, sp_count)),
            dma((sp_count,)),
            dma((sp_count,)),
            dma((len(groups), tp_count - 1)),
            dma((len(groups), tp_count - 1)),
            dma((sp_count,)),
            dma((sp_count,)),
            dma((tp_count - 1,)),
            dma((tp_count - 1,)),
        ],
        compiler_params=pltpu.CompilerParams(
            collective_id=0, has_side_effects=True, vmem_limit_bytes=60 * 1024 * 1024
        ),
    )(ids, group, weight, rates, keys, values, cot, inp, gate, up, down)


def on_device(
    cotangent,
    moe_input,
    expert_ids,
    group_weight,
    expert_weight,
    mixer_out,
    queries,
    key_vectors,
    value_vectors,
    decay_rates,
    proj_weight,
    gate_weight,
    up_weight,
    down_weight,
):
    exact = lax.Precision.HIGHEST
    sp_count = lax.axis_size("sp")
    tp_count = lax.axis_size("tp")
    me = lax.axis_index("sp")
    local_experts = gate_weight.shape[0]
    experts_all = local_experts * sp_count
    rows_here, model_width = cotangent.shape
    top_count = expert_ids.shape[1]
    capacity = 3 * top_count * rows_here // (2 * experts_all)

    heads_here, length = decay_rates.shape
    query_full = queries.astype(jnp.float32).reshape(heads_here, -1, length)
    key_full = key_vectors.astype(jnp.float32).reshape(heads_here, -1, length)
    value_full = value_vectors.astype(jnp.float32).reshape(heads_here, -1, length)
    key_size = query_full.shape[1]
    value_size = value_full.shape[1]
    score_scale = key_size ** (-0.5)
    place = jnp.arange(length, dtype=jnp.int32)
    prefix = jnp.dot(
        decay_rates, (place[:, None] <= place[None, :]).astype(jnp.float32), precision=exact
    )
    ending = prefix[:, -1:]
    mixing = score_scale * jnp.exp(-jnp.abs(prefix[:, :, None] - prefix[:, None, :]))
    toward_end = jnp.exp(prefix - ending)
    from_start = jnp.exp(-prefix)
    both_weights = jnp.stack([toward_end, from_start])
    resid_grad, key_states, grad_gate, grad_up, grad_down = experts(
        expert_ids.T,
        group_weight[None, :],
        expert_weight.T,
        decay_rates,
        key_vectors,
        value_vectors,
        cotangent,
        moe_input,
        gate_weight,
        up_weight,
        down_weight,
        capacity,
        sp_count,
        tp_count,
    )
    grad_gate, grad_up, grad_down = grad_gate[None], grad_up[None], grad_down[None]
    key_states = key_states.reshape(sp_count, heads_here, -1, value_size)

    proj_part = lax.dot_general(
        resid_grad, mixer_out, (((0,), (0,)), ((), ())), preferred_element_type=jnp.float32
    ).astype(jnp.bfloat16)
    out_grad = lax.dot_general(
        proj_weight, resid_grad, (((0,), (1,)), ((), ())), preferred_element_type=jnp.float32
    ).reshape(heads_here, -1, length)
    query_state = jnp.einsum(
        "whkl,hvl->whkv", query_full[None] * both_weights[:, :, None, :], out_grad, precision=exact
    )
    block = jnp.arange(sp_count, dtype=jnp.int32)
    query_state = query_state.astype(jnp.bfloat16).transpose(0, 2, 1, 3)
    query_state = query_state.reshape(2, key_size, heads_here * value_size)
    sent = jnp.concatenate(
        [
            proj_part.reshape(sp_count, -1, heads_here * value_size),
            jnp.where((block > me)[:, None, None], query_state[:1], query_state[1:]),
        ],
        axis=1,
    )
    shared = lax.all_to_all(sent, "sp", split_axis=0, concat_axis=0, tiled=True)
    shared = shared.astype(jnp.float32)
    proj_rows = model_width // sp_count
    grad_proj = jnp.sum(shared[:, :proj_rows], axis=0)
    query_states = shared[:, proj_rows:].reshape(sp_count, key_size, heads_here, value_size)
    query_states = query_states.transpose(0, 2, 1, 3)

    totals = key_states[:, :, key_size, 0]
    low_between = (block[None, :] > block[:, None]) & (block[None, :] < me)
    high_between = (block[None, :] < block[:, None]) & (block[None, :] > me)
    low_decay = jnp.exp(-jnp.sum(jnp.where(low_between[:, :, None], totals[None], 0.0), axis=1))
    high_decay = jnp.exp(-jnp.sum(jnp.where(high_between[:, :, None], totals[None], 0.0), axis=1))
    low_decay = jnp.where((block < me)[:, None], low_decay, 0.0)
    high_decay = jnp.where((block > me)[:, None], high_decay, 0.0)
    both_decays = jnp.stack([low_decay, high_decay])[:, :, :, None, None]
    key_carried = jnp.sum(both_decays * key_states[None, :, :, :key_size], axis=1)
    query_carried = jnp.sum(both_decays * query_states[None], axis=1)

    scores = mixing * jnp.einsum("hkt,hks->hts", query_full, key_full, precision=exact)
    score_grad = mixing * jnp.einsum("hvt,hvs->hts", out_grad, value_full, precision=exact)
    query_grad = jnp.einsum("hks,hts->hkt", key_full, score_grad, precision=exact)
    key_grad = jnp.einsum("hkt,hts->hks", query_full, score_grad, precision=exact)
    value_grad = jnp.einsum("hvt,hts->hvs", out_grad, scores, precision=exact)
    reach = score_scale * jnp.stack([from_start, toward_end])
    out_reach = out_grad[None] * reach[:, :, None, :]
    value_reach = value_full[None] * reach[:, :, None, :]
    key_reach = key_full[None] * reach[:, :, None, :]
    query_grad = query_grad + jnp.einsum("whvl,whkv->hkl", out_reach, key_carried, precision=exact)
    key_grad = key_grad + jnp.einsum("whvl,whkv->hkl", value_reach, query_carried, precision=exact)
    value_grad = value_grad + jnp.einsum("whkl,whkv->hvl", key_reach, query_carried, precision=exact)
    return (
        grad_gate,
        grad_up,
        grad_down,
        grad_proj,
        query_grad.reshape(heads_here * key_size, length),
        key_grad.reshape(heads_here * key_size, length),
        value_grad.reshape(heads_here * value_size, length),
    )


def solution(mesh):
    return jax.shard_map(
        on_device,
        mesh=mesh,
        in_specs=(
            P("sp", None),
            P("sp", None),
            P("sp", None),
            P("sp"),
            P("sp", None),
            P("sp", "tp"),
            P("tp", "sp"),
            P("tp", "sp"),
            P("tp", "sp"),
            P("tp", "sp"),
            P(None, "tp"),
            P("sp", None, "tp"),
            P("sp", None, "tp"),
            P("sp", "tp", None),
        ),
        out_specs=(
            P("sp", None, "tp"),
            P("sp", None, "tp"),
            P("sp", "tp", None),
            P("sp", "tp"),
            P("tp", "sp"),
            P("tp", "sp"),
            P("tp", "sp"),
        ),
        check_vma=False,
    )
```

time: 122 us -> 113 us (0.926)
  matrix products: 30.2 us -> 8.56 us
  waiting for transfers between devices: 0.01 us -> 14.8 us
  other arithmetic: 5.75 us -> 3.47 us
  Pallas kernels: 71.7 us -> 73.4 us
  local copies, waits for them, and re-layouts: 9.15 us -> 7.8 us
    dot_general x8 -> x0, matrix products: 19.5 us -> none  [the longest x1 4.24 us: on_device(): jnp.einsum('secd,secf->edf', inp_blocks, gate_grad, preferred_element_typ...]
    all_to_all x1, waiting for transfers between devices: 0.01 us -> 14.8 us  [on_device(): shared = lax.all_to_all(sent, 'sp', split_axis=0, concat_axis=0, tiled=True)]
    pallas_call x2 -> x1, Pallas kernels: 71.7 us -> 73.4 us  [experts(): pl.pallas_call(functools.partial(experts_kernel, sp_count, tp_count, grou...]
    unnamed x48 -> x27, local copies, waits for them, and re-layouts: 4.69 us -> 6.19 us
    broadcast_in_dim x1 -> x0, local copies, waits for them, and re-layouts: 1.39 us -> none  [on_device(): group_weight[:, None]]
    slice x1, local copies, waits for them, and re-layouts: 1.41 us -> 0.14 us  [on_device(): totals = key_states[:, :, key_size, 0]]
  transfers between devices with their start and end apart: 1 -> 1, of which waited for: 0 -> 1; matrix products, arithmetic and copies ran while one was open for 17% -> 3% of each run, Pallas kernels for 0% -> 0%
where the time goes in v1:
time: 113 us
  Pallas kernels  73.4 us (65%)
  waiting for transfers between devices  14.8 us (13%)
  matrix products  8.56 us (8%)
  local copies, waits for them, and re-layouts  7.8 us (7%)
  starting transfers between devices  3.54 us (3%)
  other arithmetic  3.47 us (3%)
    pallas_call x1, Pallas kernels, experts(): pl.pallas_call(functools.partial(experts_kernel, sp_count, tp_count, grou...  73.4 us
    all_to_all x1, waiting for transfers between devices, on_device(): shared = lax.all_to_all(sent, 'sp', split_axis=0, concat_axis=0, tiled=True)  14.8 us
    unnamed x27, local copies, waits for them, and re-layouts  6.19 us
    all_to_all x1, starting transfers between devices, on_device(): shared = lax.all_to_all(sent, 'sp', split_axis=0, concat_axis=0, tiled=True)  3.54 us
  transfers between devices with their start and end apart: 1, of which 1 were waited for; matrix products, arithmetic and copies ran while one was open for 3% of the time, Pallas kernels for 0%

profile of v1, /device:TPU:0, one launch (start us, length us, event | category | flops | bytes accessed | tf_op | source)
XLA Modules:
  0.0 112.6 jit_solution(3883555044057862855)
XLA Ops:
  0.6 0.0 copy-start
  0.7 0.8 fusion.12
  1.5 0.6 slice.23
  2.1 0.7 fusion.20
  2.8 0.7 convert_element_type.26
  3.5 0.0 copy-start.11
  3.5 73.4 %shard_map.189 = (bf16[128,2048]{1,0:T(8,128)(2,1)}, f32[8,72,128]{2,1,0:T(8,128)}, bf16[2048,512]{1,0:T(8,128)(2,1)}, bf16[2048,512]{1,0:T(8,128)(2,1)}, bf16[512,2048]{1,0:T(8,128)(2,1)}) custom-call(s32[2,128]{1,0:T(2,128)} %bitcast.91, f32[1,128]{1,0:T(1,128)} %bitcast.93, f32[2,128]{1,0:T(2,128)} %bitcast.92, f32[1,128]{1,0:T(1,128)} %rates.1, ...), custom_call_target="tpu_custom_call" | custom-call | tf_op jit(solution)/shard_map/pallas_call | solution.py:365
  77.0 0.0 copy-done
  77.0 1.3 %fusion.24 = f32[128,128]{1,0:T(8,128)S(1)} fusion(bf16[128,2048]{1,0:T(8,128)(2,1)} %get-tuple-element.15, bf16[2048,128]{1,0:T(8,128)(2,1)S(1)} %copy-done), kind=kOutput, calls=%fused_computation.58 | convolution fusion | flops 67108864 | bytes 1114112 | tf_op jit(solution)/shard_map/dot_general | solution.py:483
  78.3 0.0 copy-start.6
  78.3 0.0 copy-start.7
  78.3 0.0 copy-start.5
  78.3 0.2 fusion
  78.6 0.0 copy-done.11
  78.6 0.0 copy-start.9
  78.6 1.4 %convolution_convert_fusion = bf16[2048,128]{1,0:T(8,128)(2,1)S(1)} fusion(bf16[128,2048]{1,0:T(8,128)(2,1)} %get-tuple-element.15, bf16[128,128]{1,0:T(8,128)(2,1)S(1)} %copy-done.11), kind=kOutput, calls=%fused_computation | convolution fusion | flops 67371008 | bytes 1081344 | tf_op jit(solution)/shard_map/dot_general | solution.py:480
  80.0 0.1 broadcast_select_fusion
  80.1 0.9 pad_maximum_fusion
  80.9 3.5 %all-to-all-start = ((bf16[8,320,128]{2,1,0:T(8,128)(2,1)}), bf16[8,320,128]{2,1,0:T(8,128)(2,1)S(1)}, u32[]{:S(2)}, u32[]{:S(2)}) async-start(bf16[8,320,128]{2,1,0:T(8,128)(2,1)} %pad_maximum_fusion), calls=%async_computation | async-start | bytes 1310720 | tf_op jit(solution)/shard_map/all_to_all | solution.py:499
  84.5 0.0 copy-done.6
  84.5 0.1 slice_reduce_fusion.1
  84.7 0.2 select_reduce_fusion.1
  84.9 0.0 copy-done.7
  84.9 0.0 copy-done.5
  84.9 0.1 copy.23
  85.0 0.0 copy-done.9
  85.0 0.8 convolution_multiply_fusion
  85.8 0.2 convolution_multiply_fusion.1
  86.0 0.8 convolution_bitcast_fusion.2
  86.8 0.2 convolution_bitcast_fusion.4
  87.0 0.7 slice_bitcast_fusion
  87.7 14.8 %all-to-all-done = bf16[8,320,128]{2,1,0:T(8,128)(2,1)S(1)} async-done(((bf16[8,320,128]{2,1,0:T(8,128)(2,1)}), bf16[8,320,128]{2,1,0:T(8,128)(2,1)S(1)}, u32[]{:S(2)}, u32[]{:S(2)}) %all-to-all-start) | async-done | bytes 655392 | tf_op jit(solution)/shard_map/all_to_all | solution.py:499
  102.6 0.1 convert_element_type.30
  102.7 0.7 slice_reduce_fusion
  103.4 0.1 copy-done.4
  103.5 0.1 multiply_reduce_fusion
  103.7 0.3 convolution_bitcast_fusion
  103.9 0.0 copy-done.10
  104.0 0.9 convolution_add_fusion
  104.9 0.0 copy-done.8
  104.9 0.8 fusion.1
  105.7 0.8 fusion.2
  106.6 0.0 copy-done.3
  106.6 1.3 %copy.27 = bf16[1,2048,512]{2,1,0:T(8,128)(2,1)} copy(bf16[1,2048,512]{2,1,0:T(8,128)(2,1)S(1)} %bitcast.82) | data formatting | bytes 4194304
  107.9 1.0 copy-done.2
  108.9 1.3 %copy.28 = bf16[1,2048,512]{2,1,0:T(8,128)(2,1)} copy(bf16[1,2048,512]{2,1,0:T(8,128)(2,1)S(1)} %bitcast.81) | data formatting | bytes 4194304
  110.2 1.0 copy-done.1
  111.3 1.3 %copy.29 = bf16[1,512,2048]{2,1,0:T(8,128)(2,1)} copy(bf16[1,512,2048]{2,1,0:T(8,128)(2,1)S(1)} %bitcast.80) | data formatting | bytes 4194304
  (16 shorter events, 0.1 us)
Async XLA Ops:
  0.6 76.3 %copy-start = (bf16[2048,128]{1,0:T(8,128)(2,1)S(1)}, bf16[2048,128]{1,0:T(8,128)(2,1)}, u32[]{:S(2)}) copy-start(bf16[2048,128]{1,0:T(8,128)(2,1)} %param.24) | copy-start | bytes 1572868
  3.5 75.1 %copy-start.11 = (bf16[128,128]{1,0:T(8,128)(2,1)S(1)}, bf16[128,128]{1,0:T(8,128)(2,1)}, u32[]{:S(2)}) copy-start(bf16[128,128]{1,0:T(8,128)(2,1)} %param.19) | copy-start | bytes 98308
  78.3 6.2 %copy-start.6 = (f32[8,72,128]{2,1,0:T(8,128)S(1)}, f32[8,72,128]{2,1,0:T(8,128)}, u32[]{:S(2)}) copy-start(f32[8,72,128]{2,1,0:T(8,128)} %get-tuple-element.16) | copy-start | bytes 884740
  78.3 6.6 %copy-start.7 = (bf16[64,128]{1,0:T(8,128)(2,1)S(1)}, bf16[64,128]{1,0:T(8,128)(2,1)}, u32[]{:S(2)}) copy-start(bf16[64,128]{1,0:T(8,128)(2,1)} %keys.1) | copy-start | bytes 49156
  78.3 6.6 %copy-start.5 = (bf16[128,128]{1,0:T(8,128)(2,1)S(1)}, bf16[128,128]{1,0:T(8,128)(2,1)}, u32[]{:S(2)}) copy-start(bf16[128,128]{1,0:T(8,128)(2,1)} %values.1) | copy-start | bytes 98308
  78.6 6.4 %copy-start.9 = (bf16[64,128]{1,0:T(8,128)(2,1)S(1)}, bf16[64,128]{1,0:T(8,128)(2,1)}, u32[]{:S(2)}) copy-start(bf16[64,128]{1,0:T(8,128)(2,1)} %param.20) | copy-start | bytes 49156
  80.9 21.6 %all-to-all-start = ((bf16[8,320,128]{2,1,0:T(8,128)(2,1)}), bf16[8,320,128]{2,1,0:T(8,128)(2,1)S(1)}, u32[]{:S(2)}, u32[]{:S(2)}) async-start(bf16[8,320,128]{2,1,0:T(8,128)(2,1)} %pad_maximum_fusion), calls=%async_computation | async-start | bytes 1310720 | tf_op jit(solution)/shard_map/all_to_all | solution.py:499
  87.7 18.8 %copy-start.3 = (bf16[2048,512]{1,0:T(8,128)(2,1)S(1)}, bf16[2048,512]{1,0:T(8,128)(2,1)}, u32[]{:S(2)}) copy-start(bf16[2048,512]{1,0:T(8,128)(2,1)} %get-tuple-element.12) | copy-start | bytes 6291460
  102.6 1.0 copy-start.4
  102.6 1.4 %copy-start.10 = (f32[128,128]{1,0:T(8,128)S(1)}, f32[128,128]{1,0:T(8,128)}, u32[]{:S(2)}) copy-start(f32[128,128]{1,0:T(8,128)} %convolution_multiply_fusion) | copy-start | bytes 196612
  102.6 2.3 %copy-start.8 = (f32[64,128]{1,0:T(8,128)S(1)}, f32[64,128]{1,0:T(8,128)}, u32[]{:S(2)}) copy-start(f32[64,128]{1,0:T(8,128)} %convolution_bitcast_fusion.2) | copy-start | bytes 98308
  106.6 2.3 %copy-start.2 = (bf16[2048,512]{1,0:T(8,128)(2,1)S(1)}, bf16[2048,512]{1,0:T(8,128)(2,1)}, u32[]{:S(2)}) copy-start(bf16[2048,512]{1,0:T(8,128)(2,1)} %get-tuple-element.13) | copy-start | bytes 6291460
  108.9 2.3 %copy-start.1 = (bf16[512,2048]{1,0:T(8,128)(2,1)S(1)}, bf16[512,2048]{1,0:T(8,128)(2,1)}, u32[]{:S(2)}) copy-start(bf16[512,2048]{1,0:T(8,128)(2,1)} %get-tuple-element.14) | copy-start | bytes 6291460

commit v2 on v1

v2 whole, which is shorter than its diff:
```python
import functools

import jax
import jax.numpy as jnp
from jax import lax
from jax.experimental import pallas as pl
from jax.experimental.pallas import tpu as pltpu
from jax.sharding import PartitionSpec as P

MESH = pl.DeviceIdType.MESH
VMEM = pl.BlockSpec(memory_space=pltpu.VMEM)
ANY = pl.BlockSpec(memory_space=pl.ANY)


def partner(place, k, count):
    if k == 0:
        return place
    out = 0
    bit = 1
    while bit < count:
        b = lax.rem(place // bit, 2)
        out = out + bit * ((1 - b) if k & bit else b)
        bit *= 2
    return out


def remote(src, dst, send_sem, recv_sem, sp_place, tp_place):
    return pltpu.make_async_remote_copy(
        src_ref=src,
        dst_ref=dst,
        send_sem=send_sem,
        recv_sem=recv_sem,
        device_id={"sp": sp_place, "tp": tp_place},
        device_id_type=MESH,
    )


def state_side(here, there, count):
    return (here + count - there) // count


def dot(a, b, a_dim, b_dim):
    return lax.dot_general(
        a, b, (((a_dim,), (b_dim,)), ((), ())), preferred_element_type=jnp.float32
    )


def experts_kernel(
    sp_count, tp_count, groups,
    ids, group, weight, rates, queries, keys, values, mixer, cot_hbm, inp_hbm, gate_hbm, up_hbm, down_hbm, proj_hbm,
    grad_gate, grad_up, grad_down, grad_proj, grad_queries, grad_keys, grad_values,
    cot, inp, w_gate, w_up, w_down, w_proj, picks, either, scaled, z_src, pair_src, rows, state, state_all, resid,
    scores, mixing, reaches, key_carried, proj, pair_in, proj_out, proj_in, query_out, query_all,
    hidden, gate_grad, up_grad, part, own_part, summed_in, outgoing, returned,
    load_sem, send_z, recv_z, send_xy, recv_xy, send_far, recv_far, send_state, recv_state,
    send_rs, recv_rs, send_back, recv_back, send_ag, recv_ag, send_pair, recv_pair, send_proj, recv_proj,
    send_query, recv_query,
):
    me = lax.axis_index("sp")
    q = lax.axis_index("tp")
    tokens, model_width = cot.shape
    width = model_width // tp_count
    block_rows = rows.shape[2]
    hidden_width = w_gate.shape[1]
    square = tp_count == 4
    at = [partner(me, k, sp_count) for k in range(sp_count)]
    peer = [partner(q, m, tp_count) for m in range(tp_count)]

    def columns(place):
        return pl.ds(pl.multiple_of(place * width, width), width)

    mine = columns(q)
    loads = []
    for i, (src, dst) in enumerate(
        (
            (cot_hbm, cot),
            (inp_hbm, inp),
            (gate_hbm.at[0], w_gate),
            (up_hbm.at[0], w_up),
            (down_hbm.at[0], w_down),
            (proj_hbm, w_proj),
        )
    ):
        copy = pltpu.make_async_copy(src, dst, load_sem.at[i])
        copy.start()
        loads.append(copy)

    barrier = pltpu.get_barrier_semaphore()
    for k in range(1, sp_count):
        pl.semaphore_signal(
            barrier, inc=1, device_id={"sp": at[k], "tp": q}, device_id_type=MESH
        )
    for m in range(1, tp_count):
        pl.semaphore_signal(
            barrier, inc=1, device_id={"sp": me, "tp": peer[m]}, device_id_type=MESH
        )

    with jax.named_scope("slots"):
        top_count = ids.shape[0]
        expert = lax.broadcasted_iota(jnp.int32, (sp_count, tokens), 0)
        named = [(ids[j : j + 1, :] == expert).astype(jnp.float32) for j in range(top_count)]
        earlier = lax.broadcasted_iota(jnp.int32, (tokens, tokens), 0) < lax.broadcasted_iota(
            jnp.int32, (tokens, tokens), 1
        )
        before = jnp.dot(
            sum(named).astype(jnp.bfloat16),
            earlier.astype(jnp.float32).astype(jnp.bfloat16),
            preferred_element_type=jnp.float32,
        )
        slots = []
        route = jnp.zeros((8, tokens), jnp.float32)
        lane_of = lax.broadcasted_iota(jnp.int32, (8, tokens), 0)
        for j in range(top_count):
            rank = jnp.sum(named[j] * before, axis=0, keepdims=True).astype(jnp.int32)
            before = before + named[j]
            slots.append(ids[j : j + 1, :] * block_rows + rank)
            route = jnp.where(lane_of == j, group[...] * weight[j : j + 1, :], route)
        route = jnp.transpose(route)
        row_of = lax.broadcasted_iota(jnp.int32, (block_rows, tokens), 0)
        for k in range(sp_count):
            here = pl.ds(k * block_rows, block_rows)
            pick = [(s == row_of + at[k] * block_rows).astype(jnp.float32) for s in slots]
            for j in range(top_count):
                picks[here, j * tokens : (j + 1) * tokens] = pick[j].astype(jnp.bfloat16)
            either[here, :] = sum(pick).astype(jnp.bfloat16)

    with jax.named_scope("pack"):
        loads[0].wait()
        loads[1].wait()
        cot_mine = cot[:, mine].astype(jnp.float32)
        scaled_mine = jnp.concatenate(
            [(cot_mine * route[:, j : j + 1]).astype(jnp.bfloat16) for j in range(top_count)], axis=0
        )
        first = 2 * block_rows
        cot_out = jnp.dot(picks[first:, :], scaled_mine, preferred_element_type=jnp.float32)
        inp_out = jnp.dot(either[first:, :], inp[:, mine], preferred_element_type=jnp.float32)
        for k in range(2, sp_count):
            here = slice((k - 2) * block_rows, (k - 1) * block_rows)
            z_src[k, 0] = cot_out[here].astype(z_src.dtype)
            z_src[k, 1] = inp_out[here].astype(z_src.dtype)
    with jax.named_scope("barrier"):
        pl.semaphore_wait(barrier, sp_count - 1 + tp_count - 1)

    waits = []

    def send(copy):
        copy.start()
        waits.append(copy)

    for k in range(2, sp_count):
        send(remote(z_src.at[k], rows.at[:, k, :, mine], send_z.at[k], recv_z.at[k], at[k], q))

    with jax.named_scope("near"):
        cot_all = cot[...].astype(jnp.float32)
        for j in range(top_count):
            scaled[j * tokens : (j + 1) * tokens, :] = (cot_all * route[:, j : j + 1]).astype(scaled.dtype)
        cot_out = jnp.dot(picks[:first, :], scaled[...], preferred_element_type=jnp.float32)
        inp_out = jnp.dot(either[:first, :], inp[...], preferred_element_type=jnp.float32)
        pair_src[0] = cot_out[block_rows:].astype(pair_src.dtype)
        pair_src[1] = inp_out[block_rows:].astype(pair_src.dtype)
        send(remote(pair_src, rows.at[:, 1], send_z.at[1], recv_z.at[1], at[1], q))
        rows[0, 0] = cot_out[:block_rows].astype(rows.dtype)
        rows[1, 0] = inp_out[:block_rows].astype(rows.dtype)

    exact = lax.Precision.HIGHEST
    heads, length = rates.shape
    key_size = keys.shape[0] // heads
    value_size = values.shape[0] // heads
    score_scale = key_size ** (-0.5)

    def exact_dot(a, b, a_dim, b_dim):
        return lax.dot_general(
            a,
            b,
            (((a_dim,), (b_dim,)), ((), ())),
            precision=exact,
            preferred_element_type=jnp.float32,
        )

    def key_part(h):
        return slice(h * key_size, (h + 1) * key_size)

    def value_part(h):
        return slice(h * value_size, (h + 1) * value_size)

    def reach_part(h, side):
        return slice(8 * h + side, 8 * h + side + 1)

    with jax.named_scope("states"):
        upto = lax.broadcasted_iota(jnp.int32, (length, length), 0) <= lax.broadcasted_iota(
            jnp.int32, (length, length), 1
        )
        for h in range(heads):
            rate = jnp.broadcast_to(rates[h : h + 1, :], (8, length))
            prefixes = exact_dot(rate, upto.astype(jnp.float32), 1, 0)
            prefix = prefixes[0:1]
            ending = prefix[:, length - 1 : length]
            gap = jnp.transpose(prefixes)[:, 0:1] - prefix
            mixing[h] = score_scale * jnp.exp(-jnp.abs(gap))
            key = keys[key_part(h), :].astype(jnp.float32)
            value = values[value_part(h), :].astype(jnp.float32)
            top = h * (key_size + 8)
            for side, reach in enumerate((jnp.exp(prefix - ending), jnp.exp(-prefix))):
                reaches[reach_part(h, side), :] = reach
                state[side, top : top + key_size, :] = exact_dot(key * reach, value, 1, 1)
                state[side, top + key_size : top + key_size + 8, :] = jnp.broadcast_to(
                    ending, (8, value_size)
                )
        state_all[me] = state[0]
        query_all[me] = jnp.zeros(query_all.shape[1:], query_all.dtype)
        for k in range(1, sp_count):
            send(
                remote(
                    state.at[state_side(me, at[k], sp_count)],
                    state_all.at[me],
                    send_state.at[k],
                    recv_state.at[k],
                    at[k],
                    q,
                )
            )

    def score_stage():
        for h in range(heads):
            query = queries[key_part(h), :].astype(jnp.float32)
            key = keys[key_part(h), :].astype(jnp.float32)
            scores[h] = mixing[h] * exact_dot(query, key, 0, 0)

    def decays(h):
        total_at = h * (key_size + 8) + key_size
        low, high = [None] * sp_count, [None] * sp_count
        totals = [state_all[b, total_at : total_at + 1, :] for b in range(sp_count)]
        run = jnp.zeros((1, value_size), jnp.float32)
        for b in reversed(range(sp_count)):
            low[b] = jnp.where(b < me, jnp.exp(-run), 0.0)
            run = run + jnp.where(b < me, totals[b], 0.0)
        run = jnp.zeros((1, value_size), jnp.float32)
        for b in range(sp_count):
            high[b] = jnp.where(b > me, jnp.exp(-run), 0.0)
            run = run + jnp.where(b > me, totals[b], 0.0)
        return low, high

    def carry_stage():
        for k in range(1, sp_count):
            piece = state_all.at[at[k]]
            remote(piece, piece, send_state.at[k], recv_state.at[k], me, q).wait_recv()
        for h in range(heads):
            top = h * (key_size + 8)
            for side, decay in enumerate(decays(h)):
                total = jnp.zeros((key_size, value_size), jnp.float32)
                for b in range(sp_count):
                    total = total + decay[b] * state_all[b, top : top + key_size, :]
                key_carried[h, :, side * value_size : (side + 1) * value_size] = total

    def land(g):
        for k in range(*groups[g]):
            if k < 2:
                continue
            piece = rows.at[:, k, :, mine]
            remote(z_src.at[k], piece, send_z.at[k], recv_z.at[k], me, q).wait_recv()
            for m in range(1, tp_count):
                if square and m == 3:
                    continue
                send(
                    remote(piece, piece, send_xy.at[k, m - 1], recv_xy.at[k, m - 1], me, peer[m])
                )

    def relay(g):
        for k in range(*groups[g]):
            if k < 2:
                continue
            for m in range(1, tp_count):
                if square and m == 3:
                    continue
                piece = rows.at[:, k, :, columns(peer[m])]
                remote(piece, piece, send_xy.at[k, m - 1], recv_xy.at[k, m - 1], me, q).wait_recv()
                if square:
                    a = m - 1
                    half = rows.at[a, k, :, columns(peer[m])]
                    send(
                        remote(half, half, send_far.at[a, k], recv_far.at[a, k], me, peer[3 - m])
                    )

    def settle(g):
        for k in range(*groups[g]):
            if k == 1:
                remote(pair_src, rows.at[:, 1], send_z.at[1], recv_z.at[1], me, q).wait_recv()
            if k >= 2 and square:
                for a in range(2):
                    piece = rows.at[a, k, :, columns(peer[3])]
                    remote(piece, piece, send_far.at[a, k], recv_far.at[a, k], me, q).wait_recv()

    def forward(g):
        low, high = groups[g]
        count = high - low
        size = count * block_rows
        here = slice(low * block_rows, high * block_rows)
        got = rows[1, low:high].reshape(size, model_width)
        gate_pre = jnp.dot(got, w_gate[...], preferred_element_type=jnp.float32)
        up_pre = jnp.dot(got, w_up[...], preferred_element_type=jnp.float32)
        sigmoid_gate = jax.nn.sigmoid(gate_pre)
        silu_gate = gate_pre * sigmoid_gate
        hidden[here, :] = (silu_gate * up_pre).astype(hidden.dtype)
        got = rows[0, low:high].reshape(size, model_width)
        hidden_grad = dot(got, w_down[...], 1, 1)
        gate_rows = (
            hidden_grad * up_pre * sigmoid_gate * (1.0 + gate_pre * (1.0 - sigmoid_gate))
        ).astype(jnp.bfloat16)
        up_rows = (hidden_grad * silu_gate).astype(jnp.bfloat16)
        gate_grad[here, :] = gate_rows
        up_grad[here, :] = up_rows
        for m in list(range(tp_count - 1, 0, -1)) + [0]:
            theirs = columns(peer[m])
            partial = dot(gate_rows, w_gate[theirs, :], 1, 1) + dot(up_rows, w_up[theirs, :], 1, 1)
            partial = partial.reshape(count, block_rows, width)
            if m == 0:
                own_part[low:high] = partial
            else:
                part[m - 1, low:high] = partial.astype(part.dtype)
                send(
                    remote(
                        part.at[m - 1, pl.ds(low, count)],
                        summed_in.at[m - 1, pl.ds(low, count)],
                        send_rs.at[g, m - 1],
                        recv_rs.at[g, m - 1],
                        me,
                        peer[m],
                    )
                )

    def give_back(g):
        low, high = groups[g]
        count = high - low
        total = own_part[low:high]
        for m in range(1, tp_count):
            piece = summed_in.at[m - 1, pl.ds(low, count)]
            remote(piece, piece, send_rs.at[g, m - 1], recv_rs.at[g, m - 1], me, q).wait_recv()
            total = total + summed_in[m - 1, low:high].astype(jnp.float32)
        total = total.astype(outgoing.dtype)
        for k in range(low, high):
            if k == 0:
                returned[0] = total[0]
            else:
                outgoing[k] = total[k - low]
                send(
                    remote(
                        outgoing.at[k], returned.at[k], send_back.at[k], recv_back.at[k], at[k], q
                    )
                )

    all_rows = sp_count * block_rows

    def down_grads():
        got = rows[0].reshape(all_rows, model_width)
        for m in range(tp_count):
            cut = slice(m * width, (m + 1) * width)
            grad_down[:, cut] = dot(hidden[...], got[:, cut], 0, 0).astype(grad_down.dtype)

    def input_grads(grads, out):
        for m in range(tp_count):
            cut = slice(m * width, (m + 1) * width)
            got = rows[1, :, :, cut].reshape(all_rows, width)
            out[cut, :] = dot(got, grads[...], 0, 0).astype(out.dtype)

    count = len(groups)
    with jax.named_scope("land#g=0"):
        land(0)
        land(1)
        relay(0)
    with jax.named_scope("weights"):
        for load in loads[2:5]:
            load.wait()
    with jax.named_scope("settle#g=0"):
        settle(0)
    with jax.named_scope("forward#g=0"):
        forward(0)
    for g in range(1, count):
        with jax.named_scope(f"relay#g={g}"):
            relay(g)
        if g + 1 < count:
            with jax.named_scope(f"land#g={g + 1}"):
                land(g + 1)
        elif g >= 2:
            with jax.named_scope("give#g=0"):
                give_back(0)
        with jax.named_scope(f"settle#g={g}"):
            settle(g)
        with jax.named_scope(f"forward#g={g}"):
            forward(g)
    for g in range(0 if count <= 2 else 1, count - 1):
        with jax.named_scope(f"give#g={g}"):
            give_back(g)
    with jax.named_scope("grad_down"):
        down_grads()
    with jax.named_scope(f"give#g={count - 1}"):
        give_back(count - 1)
    with jax.named_scope("grad_gate"):
        input_grads(gate_grad, grad_gate)
    with jax.named_scope("carry"):
        score_stage()
        carry_stage()
    with jax.named_scope("back"):
        for k in range(1, sp_count):
            remote(
                outgoing.at[k], returned.at[k], send_back.at[k], recv_back.at[k], me, q
            ).wait_recv()
    with jax.named_scope("combine"):
        total = dot(either[...], returned[...].reshape(all_rows, width), 0, 0)
        resid[:, mine] = (cot[:, mine].astype(jnp.float32) + total).astype(resid.dtype)
        piece = resid.at[:, mine]
        for m in range(tp_count - 1, 0, -1):
            send(remote(piece, piece, send_ag.at[m - 1], recv_ag.at[m - 1], me, peer[m]))

    core = lax.rem(me, 2)
    chip_rows = 2 * proj.shape[2]
    chips_here = width // chip_rows

    def project(m):
        piece = resid[:, columns(peer[m])]
        weights = w_proj[columns(peer[m]), :]
        part_here = dot(piece, mixer[...], 0, 0)
        chips = pl.ds(peer[m] * chips_here, chips_here)
        proj[chips] = part_here.reshape((chips_here,) + proj.shape[1:])
        send(
            remote(
                proj.at[chips, 1 - core],
                pair_in.at[chips],
                send_pair.at[m],
                recv_pair.at[m],
                at[1],
                q,
            )
        )
        return dot(weights, piece, 0, 1)

    with jax.named_scope("project#m=0"):
        loads[5].wait()
        out_grad = project(0)
    with jax.named_scope("grad_up"):
        input_grads(up_grad, grad_up)
    for m in range(1, tp_count):
        with jax.named_scope(f"gather#m={m}"):
            piece = resid.at[:, columns(peer[m])]
            remote(piece, piece, send_ag.at[m - 1], recv_ag.at[m - 1], me, q).wait_recv()
        with jax.named_scope(f"project#m={m}"):
            out_grad = out_grad + project(m)
    with jax.named_scope("query_states"):
        for h in range(heads):
            query = queries[key_part(h), :].astype(jnp.float32)
            for side in range(2):
                seen = exact_dot(query * reaches[reach_part(h, side), :], out_grad[value_part(h)], 1, 1)
                query_out[side, key_part(h), :] = seen.astype(query_out.dtype)
        for k in reversed(range(1, sp_count)):
            send(
                remote(
                    query_out.at[state_side(me, at[k], sp_count)],
                    query_all.at[me],
                    send_query.at[k],
                    recv_query.at[k],
                    at[k],
                    q,
                )
            )
    with jax.named_scope("pair"):
        for m in range(tp_count):
            chips = pl.ds(peer[m] * chips_here, chips_here)
            remote(
                proj.at[chips, 1 - core], pair_in.at[chips], send_pair.at[m], recv_pair.at[m], me, q
            ).wait_recv()
        for k in reversed(range(2, sp_count, 2)):
            chip = at[k] // 2
            proj_out[k // 2] = (proj[chip, core] + pair_in[chip]).astype(proj_out.dtype)
            send(
                remote(
                    proj_out.at[k // 2],
                    proj_in.at[k // 2],
                    send_proj.at[k // 2],
                    recv_proj.at[k // 2],
                    at[k],
                    q,
                )
            )
        chip = me // 2
        proj_total = proj[chip, core] + pair_in[chip]
    with jax.named_scope("retention"):
        for h in range(heads):
            query = queries[key_part(h), :].astype(jnp.float32)
            key = keys[key_part(h), :].astype(jnp.float32)
            value = values[value_part(h), :].astype(jnp.float32)
            grad = out_grad[value_part(h)]
            score_grad = mixing[h] * exact_dot(grad, value, 0, 0)
            to_end = score_scale * reaches[reach_part(h, 0), :]
            from_start = score_scale * reaches[reach_part(h, 1), :]
            out_reach = jnp.concatenate([grad * from_start, grad * to_end], axis=0)
            grad_queries[key_part(h), :] = exact_dot(key, score_grad, 1, 1) + exact_dot(
                key_carried[h], out_reach, 1, 0
            )
            grad_keys[key_part(h), :] = exact_dot(query, score_grad, 1, 0)
            grad_values[value_part(h), :] = exact_dot(grad, scores[h], 1, 0)
    with jax.named_scope("query_wait"):
        for k in range(1, sp_count):
            piece = query_all.at[at[k]]
            remote(piece, piece, send_query.at[k], recv_query.at[k], me, q).wait_recv()
    with jax.named_scope("finish"):
        for h in range(heads):
            key = keys[key_part(h), :].astype(jnp.float32)
            value = values[value_part(h), :].astype(jnp.float32)
            to_end = score_scale * reaches[reach_part(h, 0), :]
            from_start = score_scale * reaches[reach_part(h, 1), :]
            carried = []
            for decay in decays(h):
                total = jnp.zeros((key_size, value_size), jnp.float32)
                for b in range(sp_count):
                    total = total + decay[b] * query_all[b, key_part(h), :].astype(jnp.float32)
                carried.append(total)
            value_reach = jnp.concatenate([value * from_start, value * to_end], axis=0)
            key_reach = jnp.concatenate([key * from_start, key * to_end], axis=0)
            grad_keys[key_part(h), :] = grad_keys[key_part(h), :] + exact_dot(
                jnp.concatenate(carried, axis=1), value_reach, 1, 0
            )
            grad_values[value_part(h), :] = grad_values[value_part(h), :] + exact_dot(
                jnp.concatenate(carried, axis=0), key_reach, 0, 0
            )
    with jax.named_scope("proj_wait"):
        for i in range(1, sp_count // 2):
            remote(
                proj_out.at[i], proj_in.at[i], send_proj.at[i], recv_proj.at[i], me, q
            ).wait_recv()
            proj_total = proj_total + proj_in[i].astype(jnp.float32)
        grad_proj[...] = proj_total
    for copy in waits:
        copy.wait_send()


def experts(
    ids, group, weight, rates, queries, keys, values, mixer, cot, inp, gate, up, down, proj, capacity, sp_count, tp_count
):
    tokens, model_width = cot.shape
    width = model_width // tp_count
    hidden_width = gate.shape[2]
    heads, length = rates.shape
    state_rows = keys.shape[0] + 8 * heads
    key_size = keys.shape[0] // heads
    value_size = values.shape[0] // heads
    head_columns = mixer.shape[1]
    proj_rows = model_width // sp_count
    block_rows = -(-capacity // 16) * 16
    all_rows = sp_count * block_rows
    chips = sp_count // 2
    quarter = sp_count // 4
    groups = [(i * quarter, (i + 1) * quarter) for i in range(4)]
    kind = cot.dtype
    full = jnp.float32
    dma = pltpu.SemaphoreType.DMA
    vmem = pltpu.VMEM
    return pl.pallas_call(
        functools.partial(experts_kernel, sp_count, tp_count, groups),
        out_shape=(
            vmem((model_width, hidden_width), kind),
            vmem((model_width, hidden_width), kind),
            vmem((hidden_width, model_width), kind),
            vmem((proj_rows, head_columns), full),
            vmem(queries.shape, full),
            vmem(keys.shape, full),
            vmem(values.shape, full),
        ),
        in_specs=[VMEM] * 8 + [ANY] * 6,
        out_specs=(VMEM,) * 7,
        scratch_shapes=[
            vmem((tokens, model_width), kind),
            vmem((tokens, model_width), kind),
            vmem((model_width, hidden_width), kind),
            vmem((model_width, hidden_width), kind),
            vmem((hidden_width, model_width), kind),
            vmem(proj.shape, kind),
            vmem((all_rows, ids.shape[0] * tokens), jnp.bfloat16),
            vmem((all_rows, tokens), jnp.bfloat16),
            vmem((ids.shape[0] * tokens, model_width), kind),
            vmem((sp_count, 2, block_rows, width), kind),
            vmem((2, block_rows, model_width), kind),
            vmem((2, sp_count, block_rows, model_width), kind),
            vmem((2, state_rows, value_size), full),
            vmem((sp_count, state_rows, value_size), full),
            vmem((tokens, model_width), kind),
            vmem((heads, length, length), full),
            vmem((heads, length, length), full),
            vmem((8 * heads, length), full),
            vmem((heads, key_size, 2 * value_size), full),
            vmem((chips, 2, proj_rows, head_columns), full),
            vmem((chips, proj_rows, head_columns), full),
            vmem((chips, proj_rows, head_columns), kind),
            vmem((chips, proj_rows, head_columns), kind),
            vmem((2, keys.shape[0], value_size), kind),
            vmem((sp_count, keys.shape[0], value_size), kind),
            vmem((all_rows, hidden_width), kind),
            vmem((all_rows, hidden_width), kind),
            vmem((all_rows, hidden_width), kind),
            vmem((tp_count - 1, sp_count, block_rows, width), kind),
            vmem((sp_count, block_rows, width), full),
            vmem((tp_count - 1, sp_count, block_rows, width), kind),
            vmem((sp_count, block_rows, width), kind),
            vmem((sp_count, block_rows, width), kind),
            dma((6,)),
            dma((sp_count,)),
            dma((sp_count,)),
            dma((sp_count, tp_count - 1)),
            dma((sp_count, tp_count - 1)),
            dma((2, sp_count)),
            dma((2, sp_count)),
            dma((sp_count,)),
            dma((sp_count,)),
            dma((len(groups), tp_count - 1)),
            dma((len(groups), tp_count - 1)),
            dma((sp_count,)),
            dma((sp_count,)),
            dma((tp_count - 1,)),
            dma((tp_count - 1,)),
            dma((tp_count,)),
            dma((tp_count,)),
            dma((chips,)),
            dma((chips,)),
            dma((sp_count,)),
            dma((sp_count,)),
        ],
        compiler_params=pltpu.CompilerParams(
            collective_id=0, has_side_effects=True, vmem_limit_bytes=48 * 1024 * 1024
        ),
    )(ids, group, weight, rates, queries, keys, values, mixer, cot, inp, gate, up, down, proj)


def on_device(
    cotangent,
    moe_input,
    expert_ids,
    group_weight,
    expert_weight,
    mixer_out,
    queries,
    key_vectors,
    value_vectors,
    decay_rates,
    proj_weight,
    gate_weight,
    up_weight,
    down_weight,
):
    sp_count = lax.axis_size("sp")
    tp_count = lax.axis_size("tp")
    experts_all = gate_weight.shape[0] * sp_count
    rows_here = cotangent.shape[0]
    top_count = expert_ids.shape[1]
    capacity = 3 * top_count * rows_here // (2 * experts_all)
    grad_gate, grad_up, grad_down, grad_proj, grad_queries, grad_keys, grad_values = experts(
        expert_ids.T,
        group_weight[None, :],
        expert_weight.T,
        decay_rates,
        queries,
        key_vectors,
        value_vectors,
        mixer_out,
        cotangent,
        moe_input,
        gate_weight,
        up_weight,
        down_weight,
        proj_weight,
        capacity,
        sp_count,
        tp_count,
    )
    return (
        grad_gate[None],
        grad_up[None],
        grad_down[None],
        grad_proj,
        grad_queries,
        grad_keys,
        grad_values,
    )


def solution(mesh):
    return jax.shard_map(
        on_device,
        mesh=mesh,
        in_specs=(
            P("sp", None),
            P("sp", None),
            P("sp", None),
            P("sp"),
            P("sp", None),
            P("sp", "tp"),
            P("tp", "sp"),
            P("tp", "sp"),
            P("tp", "sp"),
            P("tp", "sp"),
            P(None, "tp"),
            P("sp", None, "tp"),
            P("sp", None, "tp"),
            P("sp", "tp", None),
        ),
        out_specs=(
            P("sp", None, "tp"),
            P("sp", None, "tp"),
            P("sp", "tp", None),
            P("sp", "tp"),
            P("tp", "sp"),
            P("tp", "sp"),
            P("tp", "sp"),
        ),
        check_vma=False,
    )
```

time: 113 us -> 89.6 us (0.79)
  waiting for transfers between devices: 14.8 us -> 0 us
  Pallas kernels: 73.4 us -> 82.3 us
  matrix products: 8.56 us -> 0 us
  starting transfers between devices: 3.54 us -> 0 us
  other arithmetic: 3.47 us -> 0 us
  local copies, waits for them, and re-layouts: 7.8 us -> 6.47 us
    all_to_all x1 -> x0, waiting for transfers between devices: 14.8 us -> none  [on_device(): shared = lax.all_to_all(sent, 'sp', split_axis=0, concat_axis=0, tiled=True)]
    pallas_call x1, Pallas kernels: 73.4 us -> 82.3 us  [experts(): pl.pallas_call(functools.partial(experts_kernel, sp_count, tp_count, grou...]
    dot_general x12 -> x0, matrix products: 8.56 us -> none  [the longest x1 1.38 us: on_device(): lax.dot_general(resid_grad, mixer_out, (((0,), (0,)), ((), ())), preferre...]
    all_to_all x1 -> x0, starting transfers between devices: 3.54 us -> none  [on_device(): shared = lax.all_to_all(sent, 'sp', split_axis=0, concat_axis=0, tiled=True)]
    unnamed x27 -> x7, local copies, waits for them, and re-layouts: 6.19 us -> 6.47 us
  transfers between devices with their start and end apart: 1 -> 0, of which waited for: 1 -> 0; matrix products, arithmetic and copies ran while one was open for 3% -> 0% of each run, Pallas kernels for 0% -> 0%
where the time goes in v2:
time: 89.6 us; the launch traced here: 89.4 us
  Pallas kernels  82.3 us (92%)
  local copies, waits for them, and re-layouts  6.47 us (7%)
    pallas_call x1, Pallas kernels, experts(): pl.pallas_call(functools.partial(experts_kernel, sp_count, tp_count, grou...  82.3 us
    unnamed x7, local copies, waits for them, and re-layouts  6.47 us

profile of v2, /device:TPU:0, one launch (start us, length us, event | category | flops | bytes accessed | tf_op | source)
XLA Modules:
  0.0 89.4 jit_solution(1084502653800510160)
XLA Ops:
  0.6 82.3 %shard_map.189 = (bf16[2048,512]{1,0:T(8,128)(2,1)S(1)}, bf16[2048,512]{1,0:T(8,128)(2,1)S(1)}, bf16[512,2048]{1,0:T(8,128)(2,1)S(1)}, f32[256,128]{1,0:T(8,128)...) custom-call(s32[2,128]{1,0:T(2,128)} %bitcast.9, f32[1,128]{1,0:T(1,128)} %bitcast.11, ...), custom_call_target="tpu_custom_call" | custom-call | tf_op jit(solution)/shard_map/pallas_call | solution.py:556
  82.9 1.3 %copy.28 = bf16[1,2048,512]{2,1,0:T(8,128)(2,1)} copy(bf16[1,2048,512]{2,1,0:T(8,128)(2,1)S(1)} %bitcast.8) | data formatting | bytes 4194304
  84.2 1.3 %copy.29 = bf16[1,2048,512]{2,1,0:T(8,128)(2,1)} copy(bf16[1,2048,512]{2,1,0:T(8,128)(2,1)S(1)} %bitcast.7) | data formatting | bytes 4194304
  85.6 0.6 copy.32
  86.2 0.6 copy.33
  86.8 0.6 copy.34
  87.4 0.7 copy.31
  88.1 1.3 %copy.30 = bf16[1,512,2048]{2,1,0:T(8,128)(2,1)} copy(bf16[1,512,2048]{2,1,0:T(8,128)(2,1)S(1)} %bitcast.6) | data formatting | bytes 4194304

commit v3 on v2

--- a/solution.py
+++ b/solution.py
@@ -46,15 +46,14 @@
 
 
 def experts_kernel(
-    sp_count, tp_count, groups,
-    ids, group, weight, rates, queries, keys, values, mixer, cot_hbm, inp_hbm, gate_hbm, up_hbm, down_hbm, proj_hbm,
+    sp_count, tp_count, order, groups,
+    ids_hbm, group_hbm, weight_hbm, rates_hbm, queries_hbm, keys_hbm, values_hbm, mixer_hbm,
+    cot_hbm, inp_hbm, gate_hbm, up_hbm, down_hbm, proj_hbm,
     grad_gate, grad_up, grad_down, grad_proj, grad_queries, grad_keys, grad_values,
-    cot, inp, w_gate, w_up, w_down, w_proj, picks, either, scaled, z_src, pair_src, rows, state, state_all, resid,
+    ids, group, weight, rates, queries, keys, values, mixer, cot, inp, w_gate, w_up, w_down, w_proj, picks, either, scaled, z_src, pair_src, rows, state, state_all, resid,
     scores, mixing, reaches, key_carried, proj, pair_in, proj_out, proj_in, query_out, query_all,
-    hidden, gate_grad, up_grad, part, own_part, summed_in, outgoing, returned,
-    load_sem, send_z, recv_z, send_xy, recv_xy, send_far, recv_far, send_state, recv_state,
-    send_rs, recv_rs, send_back, recv_back, send_ag, recv_ag, send_pair, recv_pair, send_proj, recv_proj,
-    send_query, recv_query,
+    hidden, gate_grad, up_grad, part, own_part, kept, summed_in, outgoing, returned,
+    load_sem, send_sem, recv_z, recv_xy, recv_far, recv_rs, recv_hop, recv_ag, recv_all,
 ):
     me = lax.axis_index("sp")
     q = lax.axis_index("tp")
@@ -63,21 +62,35 @@
     block_rows = rows.shape[2]
     hidden_width = w_gate.shape[1]
     square = tp_count == 4
-    at = [partner(me, k, sp_count) for k in range(sp_count)]
+    at = [partner(me, k, sp_count) for k in order]
     peer = [partner(q, m, tp_count) for m in range(tp_count)]
 
     def columns(place):
         return pl.ds(pl.multiple_of(place * width, width), width)
 
     mine = columns(q)
+    halves = 2 if width == 2 * proj.shape[2] and proj.shape[2] % 128 == 0 else 1
+
+    def half_columns(place, j):
+        size = width // halves
+        return pl.ds(pl.multiple_of(place * width + j * size, size), size)
+
     loads = []
     for i, (src, dst) in enumerate(
         (
+            (ids_hbm, ids),
+            (group_hbm, group),
+            (weight_hbm, weight),
             (cot_hbm, cot),
             (inp_hbm, inp),
+            (rates_hbm, rates),
+            (keys_hbm, keys),
+            (values_hbm, values),
             (gate_hbm.at[0], w_gate),
             (up_hbm.at[0], w_up),
             (down_hbm.at[0], w_down),
+            (queries_hbm, queries),
+            (mixer_hbm, mixer),
             (proj_hbm, w_proj),
         )
     ):
@@ -96,6 +109,8 @@
         )
 
     with jax.named_scope("slots"):
+        for load in loads[:3]:
+            load.wait()
         top_count = ids.shape[0]
         expert = lax.broadcasted_iota(jnp.int32, (sp_count, tokens), 0)
         named = [(ids[j : j + 1, :] == expert).astype(jnp.float32) for j in range(top_count)]
@@ -125,8 +140,8 @@
             either[here, :] = sum(pick).astype(jnp.bfloat16)
 
     with jax.named_scope("pack"):
-        loads[0].wait()
-        loads[1].wait()
+        loads[3].wait()
+        loads[4].wait()
         cot_mine = cot[:, mine].astype(jnp.float32)
         scaled_mine = jnp.concatenate(
             [(cot_mine * route[:, j : j + 1]).astype(jnp.bfloat16) for j in range(top_count)], axis=0
@@ -141,15 +156,13 @@
     with jax.named_scope("barrier"):
         pl.semaphore_wait(barrier, sp_count - 1 + tp_count - 1)
 
-    waits = []
-
-    def send(copy):
+    pending = []
+
+    def start(copy):
         copy.start()
-        waits.append(copy)
 
     for k in range(2, sp_count):
-        send(remote(z_src.at[k], rows.at[:, k, :, mine], send_z.at[k], recv_z.at[k], at[k], q))
-
+        start(remote(z_src.at[k], rows.at[:, k, :, mine], send_sem.at[0], recv_z.at[k], at[k], q))
     with jax.named_scope("near"):
         cot_all = cot[...].astype(jnp.float32)
         for j in range(top_count):
@@ -158,7 +171,7 @@
         inp_out = jnp.dot(either[:first, :], inp[...], preferred_element_type=jnp.float32)
         pair_src[0] = cot_out[block_rows:].astype(pair_src.dtype)
         pair_src[1] = inp_out[block_rows:].astype(pair_src.dtype)
-        send(remote(pair_src, rows.at[:, 1], send_z.at[1], recv_z.at[1], at[1], q))
+        start(remote(pair_src, rows.at[:, 1], send_sem.at[1], recv_z.at[1], at[1], q))
         rows[0, 0] = cot_out[:block_rows].astype(rows.dtype)
         rows[1, 0] = inp_out[:block_rows].astype(rows.dtype)
 
@@ -187,6 +200,8 @@
         return slice(8 * h + side, 8 * h + side + 1)
 
     with jax.named_scope("states"):
+        for load in loads[5:8]:
+            load.wait()
         upto = lax.broadcasted_iota(jnp.int32, (length, length), 0) <= lax.broadcasted_iota(
             jnp.int32, (length, length), 1
         )
@@ -209,18 +224,19 @@
         state_all[me] = state[0]
         query_all[me] = jnp.zeros(query_all.shape[1:], query_all.dtype)
         for k in range(1, sp_count):
-            send(
+            start(
                 remote(
                     state.at[state_side(me, at[k], sp_count)],
                     state_all.at[me],
-                    send_state.at[k],
-                    recv_state.at[k],
+                    send_sem.at[4],
+                    recv_all.at[0],
                     at[k],
                     q,
                 )
             )
 
     def score_stage():
+        loads[11].wait()
         for h in range(heads):
             query = queries[key_part(h), :].astype(jnp.float32)
             key = keys[key_part(h), :].astype(jnp.float32)
@@ -241,9 +257,8 @@
         return low, high
 
     def carry_stage():
-        for k in range(1, sp_count):
-            piece = state_all.at[at[k]]
-            remote(piece, piece, send_state.at[k], recv_state.at[k], me, q).wait_recv()
+        piece = state_all.at[pl.ds(0, sp_count - 1)]
+        remote(piece, piece, send_sem.at[4], recv_all.at[0], me, q).wait_recv()
         for h in range(heads):
             top = h * (key_size + 8)
             for side, decay in enumerate(decays(h)):
@@ -257,12 +272,12 @@
             if k < 2:
                 continue
             piece = rows.at[:, k, :, mine]
-            remote(z_src.at[k], piece, send_z.at[k], recv_z.at[k], me, q).wait_recv()
+            remote(z_src.at[k], piece, send_sem.at[0], recv_z.at[k], me, q).wait_recv()
             for m in range(1, tp_count):
                 if square and m == 3:
                     continue
-                send(
-                    remote(piece, piece, send_xy.at[k, m - 1], recv_xy.at[k, m - 1], me, peer[m])
+                start(
+                    remote(piece, piece, send_sem.at[2], recv_xy.at[k - 2, m - 1], me, peer[m])
                 )
 
     def relay(g):
@@ -273,22 +288,22 @@
                 if square and m == 3:
                     continue
                 piece = rows.at[:, k, :, columns(peer[m])]
-                remote(piece, piece, send_xy.at[k, m - 1], recv_xy.at[k, m - 1], me, q).wait_recv()
+                remote(piece, piece, send_sem.at[2], recv_xy.at[k - 2, m - 1], me, q).wait_recv()
                 if square:
                     a = m - 1
                     half = rows.at[a, k, :, columns(peer[m])]
-                    send(
-                        remote(half, half, send_far.at[a, k], recv_far.at[a, k], me, peer[3 - m])
+                    start(
+                        remote(half, half, send_sem.at[3], recv_far.at[a, k - 2], me, peer[3 - m])
                     )
 
     def settle(g):
         for k in range(*groups[g]):
             if k == 1:
-                remote(pair_src, rows.at[:, 1], send_z.at[1], recv_z.at[1], me, q).wait_recv()
+                remote(pair_src, rows.at[:, 1], send_sem.at[1], recv_z.at[1], me, q).wait_recv()
             if k >= 2 and square:
                 for a in range(2):
                     piece = rows.at[a, k, :, columns(peer[3])]
-                    remote(piece, piece, send_far.at[a, k], recv_far.at[a, k], me, q).wait_recv()
+                    remote(piece, piece, send_sem.at[3], recv_far.at[a, k - 2], me, q).wait_recv()
 
     def forward(g):
         low, high = groups[g]
@@ -309,42 +324,107 @@
         up_rows = (hidden_grad * silu_gate).astype(jnp.bfloat16)
         gate_grad[here, :] = gate_rows
         up_grad[here, :] = up_rows
-        for m in list(range(tp_count - 1, 0, -1)) + [0]:
+
+        def partial(m):
             theirs = columns(peer[m])
-            partial = dot(gate_rows, w_gate[theirs, :], 1, 1) + dot(up_rows, w_up[theirs, :], 1, 1)
-            partial = partial.reshape(count, block_rows, width)
-            if m == 0:
-                own_part[low:high] = partial
-            else:
-                part[m - 1, low:high] = partial.astype(part.dtype)
-                send(
+            total = dot(gate_rows, w_gate[theirs, :], 1, 1) + dot(up_rows, w_up[theirs, :], 1, 1)
+            return total.reshape(count, block_rows, width)
+
+        if square:
+            half = count // 2
+            middle = low + half
+            total = partial(3).astype(part.dtype)
+            part[1, low:high] = total
+            total = partial(1)
+            part[0, low:middle] = total[:half].astype(part.dtype)
+            kept[middle:high] = total[half:]
+            pending.append(first_hop(g, 0))
+            total = partial(2)
+            part[0, middle:high] = total[half:].astype(part.dtype)
+            kept[low:middle] = total[:half]
+            pending.append(first_hop(g, 1))
+        else:
+            for m in range(tp_count - 1, 0, -1):
+                part[m - 1, low:high] = partial(m).astype(part.dtype)
+                piece = pl.ds(low, count)
+                start(
                     remote(
-                        part.at[m - 1, pl.ds(low, count)],
-                        summed_in.at[m - 1, pl.ds(low, count)],
-                        send_rs.at[g, m - 1],
+                        part.at[m - 1, piece],
+                        summed_in.at[m - 1, piece],
+                        send_sem.at[5],
                         recv_rs.at[g, m - 1],
                         me,
                         peer[m],
                     )
                 )
+        own_part[low:high] = partial(0)
+
+    def flush():
+        while pending:
+            start(pending.pop(0))
+
+    def hop_blocks(g, side):
+        low, high = groups[g]
+        half = (high - low) // 2
+        return (low, low + half) if side == 0 else (low + half, high)
+
+    def first_hop(g, side):
+        low, high = hop_blocks(g, side)
+        piece = pl.ds(low, high - low)
+        return remote(
+            part.at[pl.ds(0, 2), piece],
+            summed_in.at[pl.ds(0, 2), piece],
+            send_sem.at[5],
+            recv_rs.at[g, side],
+            me,
+            peer[1 + side],
+        )
+
+    def second_hop(g, side):
+        low, high = hop_blocks(g, side)
+        piece = pl.ds(low, high - low)
+        return remote(
+            part.at[2, piece],
+            summed_in.at[2, piece],
+            send_sem.at[6],
+            recv_hop.at[g, side],
+            me,
+            peer[2 - side],
+        )
+
+    def hop(g):
+        if not square:
+            return
+        for side in range(2):
+            low, high = hop_blocks(g, side)
+            first_hop(g, side).wait_recv()
+            total = kept[low:high] + summed_in[1, low:high].astype(jnp.float32)
+            part[2, low:high] = total.astype(part.dtype)
+            start(second_hop(g, side))
 
     def give_back(g):
         low, high = groups[g]
         count = high - low
         total = own_part[low:high]
-        for m in range(1, tp_count):
-            piece = summed_in.at[m - 1, pl.ds(low, count)]
-            remote(piece, piece, send_rs.at[g, m - 1], recv_rs.at[g, m - 1], me, q).wait_recv()
-            total = total + summed_in[m - 1, low:high].astype(jnp.float32)
+        if square:
+            for side in range(2):
+                second_hop(g, side).wait_recv()
+            total = total + summed_in[0, low:high].astype(jnp.float32)
+            total = total + summed_in[2, low:high].astype(jnp.float32)
+        else:
+            for m in range(1, tp_count):
+                piece = summed_in.at[m - 1, pl.ds(low, count)]
+                remote(piece, piece, send_sem.at[5], recv_rs.at[g, m - 1], me, q).wait_recv()
+                total = total + summed_in[m - 1, low:high].astype(jnp.float32)
         total = total.astype(outgoing.dtype)
         for k in range(low, high):
             if k == 0:
                 returned[0] = total[0]
             else:
                 outgoing[k] = total[k - low]
-                send(
+                start(
                     remote(
-                        outgoing.at[k], returned.at[k], send_back.at[k], recv_back.at[k], at[k], q
+                        outgoing.at[k], returned.at[k], send_sem.at[7], recv_all.at[1], at[k], q
                     )
                 )
 
@@ -363,87 +443,144 @@
             out[cut, :] = dot(got, grads[...], 0, 0).astype(out.dtype)
 
     count = len(groups)
+    with jax.named_scope("weights"):
+        for load in loads[8:11]:
+            load.wait()
     with jax.named_scope("land#g=0"):
         land(0)
-        land(1)
         relay(0)
-    with jax.named_scope("weights"):
-        for load in loads[2:5]:
-            load.wait()
-    with jax.named_scope("settle#g=0"):
         settle(0)
     with jax.named_scope("forward#g=0"):
         forward(0)
-    for g in range(1, count):
-        with jax.named_scope(f"relay#g={g}"):
-            relay(g)
-        if g + 1 < count:
-            with jax.named_scope(f"land#g={g + 1}"):
-                land(g + 1)
-        elif g >= 2:
-            with jax.named_scope("give#g=0"):
-                give_back(0)
-        with jax.named_scope(f"settle#g={g}"):
-            settle(g)
-        with jax.named_scope(f"forward#g={g}"):
-            forward(g)
-    for g in range(0 if count <= 2 else 1, count - 1):
-        with jax.named_scope(f"give#g={g}"):
-            give_back(g)
+    flush()
+    with jax.named_scope("land#g=1"):
+        land(1)
+    with jax.named_scope("hop#g=0"):
+        hop(0)
+    with jax.named_scope("relay#g=1"):
+        relay(1)
+    with jax.named_scope("land#g=2"):
+        land(2)
+    with jax.named_scope("settle#g=1"):
+        settle(1)
+    with jax.named_scope("forward#g=1"):
+        forward(1)
+    with jax.named_scope("relay#g=2"):
+        relay(2)
+    flush()
+    with jax.named_scope("land#g=3"):
+        land(3)
+    with jax.named_scope("settle#g=2"):
+        settle(2)
+    with jax.named_scope("forward#g=2"):
+        forward(2)
+    flush()
+    with jax.named_scope("relay#g=3"):
+        relay(3)
+    with jax.named_scope("hop#g=1"):
+        hop(1)
+    with jax.named_scope("give#g=0"):
+        give_back(0)
+    with jax.named_scope("hop#g=2"):
+        hop(2)
+    with jax.named_scope("settle#g=3"):
+        settle(3)
+    with jax.named_scope("forward#g=3"):
+        forward(3)
+    flush()
+    with jax.named_scope("give#g=1"):
+        give_back(1)
+    with jax.named_scope("give#g=2"):
+        give_back(2)
     with jax.named_scope("grad_down"):
         down_grads()
-    with jax.named_scope(f"give#g={count - 1}"):
-        give_back(count - 1)
+    with jax.named_scope("hop#g=3"):
+        hop(3)
     with jax.named_scope("grad_gate"):
         input_grads(gate_grad, grad_gate)
+    with jax.named_scope("give#g=3"):
+        give_back(3)
     with jax.named_scope("carry"):
         score_stage()
         carry_stage()
     with jax.named_scope("back"):
-        for k in range(1, sp_count):
-            remote(
-                outgoing.at[k], returned.at[k], send_back.at[k], recv_back.at[k], me, q
-            ).wait_recv()
+        piece = returned.at[pl.ds(0, sp_count - 1)]
+        remote(piece, piece, send_sem.at[7], recv_all.at[1], me, q).wait_recv()
     with jax.named_scope("combine"):
         total = dot(either[...], returned[...].reshape(all_rows, width), 0, 0)
         resid[:, mine] = (cot[:, mine].astype(jnp.float32) + total).astype(resid.dtype)
-        piece = resid.at[:, mine]
-        for m in range(tp_count - 1, 0, -1):
-            send(remote(piece, piece, send_ag.at[m - 1], recv_ag.at[m - 1], me, peer[m]))
+        for j in range(halves):
+            piece = resid.at[:, half_columns(q, j)]
+            for m in range(tp_count - 1, 0, -1):
+                start(remote(piece, piece, send_sem.at[8], recv_ag.at[m - 1, j], me, peer[m]))
 
     core = lax.rem(me, 2)
-    chip_rows = 2 * proj.shape[2]
-    chips_here = width // chip_rows
-
-    def project(m):
-        piece = resid[:, columns(peer[m])]
-        weights = w_proj[columns(peer[m]), :]
+    chips_here = width // (2 * proj.shape[2])
+
+    def project(m, j):
+        piece = resid[:, half_columns(peer[m], j)]
         part_here = dot(piece, mixer[...], 0, 0)
         chips = pl.ds(peer[m] * chips_here, chips_here)
-        proj[chips] = part_here.reshape((chips_here,) + proj.shape[1:])
-        send(
-            remote(
-                proj.at[chips, 1 - core],
-                pair_in.at[chips],
-                send_pair.at[m],
-                recv_pair.at[m],
-                at[1],
-                q,
+        if halves == 2:
+            proj[chips, j] = part_here.reshape((chips_here,) + proj.shape[2:])
+        else:
+            proj[chips] = part_here.reshape((chips_here,) + proj.shape[1:])
+        return dot(w_proj[half_columns(peer[m], j), :], piece, 0, 1)
+
+    def pair_copy():
+        return remote(
+            proj.at[:, 1 - core], pair_in, send_sem.at[9], recv_all.at[2], at[1], q
+        )
+
+    def pair_total(chip):
+        return proj[chip, core] + pair_in[chip]
+
+    def across_chips():
+        pair_copy().wait_recv()
+        for k in reversed(range(2, sp_count, 2)):
+            proj_out[k // 2] = pair_total(at[k] // 2).astype(proj_out.dtype)
+            start(
+                remote(
+                    proj_out.at[k // 2],
+                    proj_in.at[k // 2],
+                    send_sem.at[10],
+                    recv_all.at[3],
+                    at[k],
+                    q,
+                )
             )
-        )
-        return dot(weights, piece, 0, 1)
+        grad_proj[...] = pair_total(me // 2)
 
     with jax.named_scope("project#m=0"):
-        loads[5].wait()
-        out_grad = project(0)
+        loads[12].wait()
+        loads[13].wait()
+        out_grad = project(0, 0)
+        for j in range(1, halves):
+            out_grad = out_grad + project(0, j)
     with jax.named_scope("grad_up"):
         input_grads(up_grad, grad_up)
-    for m in range(1, tp_count):
-        with jax.named_scope(f"gather#m={m}"):
-            piece = resid.at[:, columns(peer[m])]
-            remote(piece, piece, send_ag.at[m - 1], recv_ag.at[m - 1], me, q).wait_recv()
-        with jax.named_scope(f"project#m={m}"):
-            out_grad = out_grad + project(m)
+    for j in range(halves):
+        for m in range(1, tp_count):
+            with jax.named_scope(f"gather#m={m}#j={j}"):
+                piece = resid.at[:, half_columns(peer[m], j)]
+                remote(piece, piece, send_sem.at[8], recv_ag.at[m - 1, j], me, q).wait_recv()
+            with jax.named_scope(f"project#m={m}#j={j}"):
+                out_grad = out_grad + project(m, j)
+        if halves == 2:
+            with jax.named_scope(f"pair#j={j}"):
+
+                @pl.when(core != j)
+                def _():
+                    pair_copy().start()
+
+                if j == 0:
+
+                    @pl.when(core == j)
+                    def _():
+                        across_chips()
+
+    if halves == 1:
+        pair_copy().start()
     with jax.named_scope("query_states"):
         for h in range(heads):
             query = queries[key_part(h), :].astype(jnp.float32)
@@ -451,37 +588,25 @@
                 seen = exact_dot(query * reaches[reach_part(h, side), :], out_grad[value_part(h)], 1, 1)
                 query_out[side, key_part(h), :] = seen.astype(query_out.dtype)
         for k in reversed(range(1, sp_count)):
-            send(
+            start(
                 remote(
                     query_out.at[state_side(me, at[k], sp_count)],
                     query_all.at[me],
-                    send_query.at[k],
-                    recv_query.at[k],
+                    send_sem.at[11],
+                    recv_all.at[4],
                     at[k],
                     q,
                 )
             )
     with jax.named_scope("pair"):
-        for m in range(tp_count):
-            chips = pl.ds(peer[m] * chips_here, chips_here)
-            remote(
-                proj.at[chips, 1 - core], pair_in.at[chips], send_pair.at[m], recv_pair.at[m], me, q
-            ).wait_recv()
-        for k in reversed(range(2, sp_count, 2)):
-            chip = at[k] // 2
-            proj_out[k // 2] = (proj[chip, core] + pair_in[chip]).astype(proj_out.dtype)
-            send(
-                remote(
-                    proj_out.at[k // 2],
-                    proj_in.at[k // 2],
-                    send_proj.at[k // 2],
-                    recv_proj.at[k // 2],
-                    at[k],
-                    q,
-                )
-            )
-        chip = me // 2
-        proj_total = proj[chip, core] + pair_in[chip]
+        if halves == 1:
+            across_chips()
+        else:
+
+            @pl.when(core == 1)
+            def _():
+                across_chips()
+
     with jax.named_scope("retention"):
         for h in range(heads):
             query = queries[key_part(h), :].astype(jnp.float32)
@@ -498,9 +623,8 @@
             grad_keys[key_part(h), :] = exact_dot(query, score_grad, 1, 0)
             grad_values[value_part(h), :] = exact_dot(grad, scores[h], 1, 0)
     with jax.named_scope("query_wait"):
-        for k in range(1, sp_count):
-            piece = query_all.at[at[k]]
-            remote(piece, piece, send_query.at[k], recv_query.at[k], me, q).wait_recv()
+        piece = query_all.at[pl.ds(0, sp_count - 1)]
+        remote(piece, piece, send_sem.at[11], recv_all.at[4], me, q).wait_recv()
     with jax.named_scope("finish"):
         for h in range(heads):
             key = keys[key_part(h), :].astype(jnp.float32)
@@ -522,14 +646,54 @@
                 jnp.concatenate(carried, axis=0), key_reach, 0, 0
             )
     with jax.named_scope("proj_wait"):
+        piece = proj_in.at[pl.ds(1, sp_count // 2 - 1)]
+        remote(piece, piece, send_sem.at[10], recv_all.at[3], me, q).wait_recv()
+        proj_total = grad_proj[...]
         for i in range(1, sp_count // 2):
-            remote(
-                proj_out.at[i], proj_in.at[i], send_proj.at[i], recv_proj.at[i], me, q
-            ).wait_recv()
             proj_total = proj_total + proj_in[i].astype(jnp.float32)
         grad_proj[...] = proj_total
-    for copy in waits:
-        copy.wait_send()
+    with jax.named_scope("sent"):
+        others = pl.ds(0, sp_count - 2)
+        crossing = 2 if square else tp_count - 1
+        sent = [
+            rows.at[:, others, :, pl.ds(0, width)],
+            pair_src,
+            rows.at[:, others, :, pl.ds(0, crossing * width)],
+            rows.at[:, others, :, pl.ds(0, width)] if square else None,
+            state_all.at[pl.ds(0, sp_count - 1)],
+            part.at[pl.ds(0, 2)] if square else part,
+            part.at[2] if square else None,
+            outgoing.at[pl.ds(0, sp_count - 1)],
+            resid.at[:, pl.ds(0, (tp_count - 1) * width)],
+            pair_in,
+            proj_out.at[pl.ds(0, sp_count // 2 - 1)],
+            query_all.at[pl.ds(0, sp_count - 1)],
+        ]
+        for i, piece in enumerate(sent):
+            if piece is not None:
+                remote(piece, piece, send_sem.at[i], recv_all.at[0], me, q).wait_send()
+
+
+def store_kernel(*refs):
+    count = (len(refs) - 1) // 2
+    copies = [
+        pltpu.make_async_copy(refs[i], refs[count + i], refs[-1].at[i]) for i in range(count)
+    ]
+    for copy in copies:
+        copy.start()
+    for copy in copies:
+        copy.wait()
+
+
+def store(arrays):
+    return pl.pallas_call(
+        store_kernel,
+        out_shape=tuple(jax.ShapeDtypeStruct(a.shape, a.dtype) for a in arrays),
+        in_specs=[VMEM] * len(arrays),
+        out_specs=(ANY,) * len(arrays),
+        scratch_shapes=[pltpu.SemaphoreType.DMA((len(arrays),))],
+        compiler_params=pltpu.CompilerParams(vmem_limit_bytes=16 * 1024 * 1024),
+    )(*arrays)
 
 
 def experts(
@@ -548,13 +712,16 @@
     all_rows = sp_count * block_rows
     chips = sp_count // 2
     quarter = sp_count // 4
+    pairs = [0, 1] + list(range(sp_count // 2 - 1, 1, -1))
+    order = [k for pair in pairs for k in (2 * pair, 2 * pair + 1)]
     groups = [(i * quarter, (i + 1) * quarter) for i in range(4)]
+    crossing = 2 if tp_count == 4 else tp_count - 1
     kind = cot.dtype
     full = jnp.float32
     dma = pltpu.SemaphoreType.DMA
     vmem = pltpu.VMEM
     return pl.pallas_call(
-        functools.partial(experts_kernel, sp_count, tp_count, groups),
+        functools.partial(experts_kernel, sp_count, tp_count, order, groups),
         out_shape=(
             vmem((model_width, hidden_width), kind),
             vmem((model_width, hidden_width), kind),
@@ -564,9 +731,17 @@
             vmem(keys.shape, full),
             vmem(values.shape, full),
         ),
-        in_specs=[VMEM] * 8 + [ANY] * 6,
+        in_specs=[ANY] * 14,
         out_specs=(VMEM,) * 7,
         scratch_shapes=[
+            vmem(ids.shape, ids.dtype),
+            vmem(group.shape, group.dtype),
+            vmem(weight.shape, weight.dtype),
+            vmem(rates.shape, rates.dtype),
+            vmem(queries.shape, queries.dtype),
+            vmem(keys.shape, keys.dtype),
+            vmem(values.shape, values.dtype),
+            vmem(mixer.shape, mixer.dtype),
             vmem((tokens, model_width), kind),
             vmem((tokens, model_width), kind),
             vmem((model_width, hidden_width), kind),
@@ -597,30 +772,19 @@
             vmem((all_rows, hidden_width), kind),
             vmem((tp_count - 1, sp_count, block_rows, width), kind),
             vmem((sp_count, block_rows, width), full),
+            vmem((sp_count, block_rows, width), full),
             vmem((tp_count - 1, sp_count, block_rows, width), kind),
             vmem((sp_count, block_rows, width), kind),
             vmem((sp_count, block_rows, width), kind),
-            dma((6,)),
+            dma((14,)),
+            dma((12,)),
             dma((sp_count,)),
-            dma((sp_count,)),
-            dma((sp_count, tp_count - 1)),
-            dma((sp_count, tp_count - 1)),
-            dma((2, sp_count)),
-            dma((2, sp_count)),
-            dma((sp_count,)),
-            dma((sp_count,)),
-            dma((len(groups), tp_count - 1)),
-            dma((len(groups), tp_count - 1)),
-            dma((sp_count,)),
-            dma((sp_count,)),
-            dma((tp_count - 1,)),
-            dma((tp_count - 1,)),
-            dma((tp_count,)),
-            dma((tp_count,)),
-            dma((chips,)),
-            dma((chips,)),
-            dma((sp_count,)),
-            dma((sp_count,)),
+            dma((sp_count - 2, crossing)),
+            dma((2, sp_count - 2)),
+            dma((len(groups), crossing)),
+            dma((len(groups), 2)),
+            dma((tp_count - 1, 2)),
+            dma((5,)),
         ],
         compiler_params=pltpu.CompilerParams(
             collective_id=0, has_side_effects=True, vmem_limit_bytes=48 * 1024 * 1024
@@ -650,7 +814,7 @@
     rows_here = cotangent.shape[0]
     top_count = expert_ids.shape[1]
     capacity = 3 * top_count * rows_here // (2 * experts_all)
-    grad_gate, grad_up, grad_down, grad_proj, grad_queries, grad_keys, grad_values = experts(
+    results = experts(
         expert_ids.T,
         group_weight[None, :],
         expert_weight.T,
@@ -669,6 +833,7 @@
         sp_count,
         tp_count,
     )
+    grad_gate, grad_up, grad_down, grad_proj, grad_queries, grad_keys, grad_values = store(results)
     return (
         grad_gate[None],
         grad_up[None],

time: 89.6 us -> 73.7 us (0.82)
  Pallas kernels: 82.3 us -> 72.9 us
  local copies, waits for them, and re-layouts: 6.47 us -> 0 us
    pallas_call x1 -> x2, Pallas kernels: 82.3 us -> 72.9 us  [the longest x1 70.2 us: experts(): pl.pallas_call(functools.partial(experts_kernel, sp_count, tp_count, orde...]
    unnamed x7 -> x0, local copies, waits for them, and re-layouts: 6.47 us -> none
where the time goes in v3:
time: 73.7 us; the launch traced here: 73.6 us
  Pallas kernels  72.9 us (99%)
    pallas_call x1, Pallas kernels, experts(): pl.pallas_call(functools.partial(experts_kernel, sp_count, tp_count, orde...  70.2 us
    pallas_call x1, Pallas kernels, store(): pl.pallas_call(store_kernel, out_shape=tuple((jax.ShapeDtypeStruct(a.shap...  2.77 us

profile of v3, /device:TPU:0, one launch (start us, length us, event | category | flops | bytes accessed | tf_op | source)
XLA Modules:
  0.0 73.6 jit_solution(4440122586471698716)
XLA Ops:
  0.6 70.2 %shard_map.189 = (bf16[2048,512]{1,0:T(8,128)(2,1)S(1)}, bf16[2048,512]{1,0:T(8,128)(2,1)S(1)}, bf16[512,2048]{1,0:T(8,128)(2,1)S(1)}, f32[256,128]{1,0:T(8,128)...) custom-call(s32[2,128]{1,0:T(2,128)} %bitcast.6, f32[1,128]{1,0:T(1,128)} %bitcast.8, ...), custom_call_target="tpu_custom_call" | custom-call | tf_op jit(solution)/shard_map/pallas_call | solution.py:723
  70.8 2.8 %shard_map.190 = (bf16[2048,512]{1,0:T(8,128)(2,1)}, bf16[2048,512]{1,0:T(8,128)(2,1)}, bf16[512,2048]{1,0:T(8,128)(2,1)}, f32[256,128]{1,0:T(8,128)}, f32[64,12...) custom-call(bf16[2048,512]{1,0:T(8,128)(2,1)S(1)} %get-tuple-element.21.refs_0_, ...), custom_call_target="tpu_custom_call" | custom-call | tf_op jit(solution)/shard_map/pallas_call | solution.py:689

commit v4 on v3

--- a/solution.py
+++ b/solution.py
@@ -50,7 +50,7 @@
     ids_hbm, group_hbm, weight_hbm, rates_hbm, queries_hbm, keys_hbm, values_hbm, mixer_hbm,
     cot_hbm, inp_hbm, gate_hbm, up_hbm, down_hbm, proj_hbm,
     grad_gate, grad_up, grad_down, grad_proj, grad_queries, grad_keys, grad_values,
-    ids, group, weight, rates, queries, keys, values, mixer, cot, inp, w_gate, w_up, w_down, w_proj, picks, either, scaled, z_src, pair_src, rows, state, state_all, resid,
+    ids, group, weight, rates, queries, keys, values, mixer, cot, inp, w_gate, w_up, w_down, w_proj, picks, either, scaled, z_src, far_src, pair_src, rows, state, state_all, resid,
     scores, mixing, reaches, key_carried, proj, pair_in, proj_out, proj_in, query_out, query_all,
     hidden, gate_grad, up_grad, part, own_part, kept, summed_in, outgoing, returned,
     load_sem, send_sem, recv_z, recv_xy, recv_far, recv_rs, recv_hop, recv_ag, recv_all,
@@ -63,6 +63,7 @@
     hidden_width = w_gate.shape[1]
     square = tp_count == 4
     at = [partner(me, k, sp_count) for k in order]
+    direct = list(range(*groups[-1])) if square else []
     peer = [partner(q, m, tp_count) for m in range(tp_count)]
 
     def columns(place):
@@ -172,6 +173,15 @@
         pair_src[0] = cot_out[block_rows:].astype(pair_src.dtype)
         pair_src[1] = inp_out[block_rows:].astype(pair_src.dtype)
         start(remote(pair_src, rows.at[:, 1], send_sem.at[1], recv_z.at[1], at[1], q))
+        if direct:
+            across = columns(peer[3])
+            here = slice(direct[0] * block_rows, (direct[-1] + 1) * block_rows)
+            cot_far = jnp.dot(picks[here, :], scaled[:, across], preferred_element_type=jnp.float32)
+            inp_far = jnp.dot(either[here, :], inp[:, across], preferred_element_type=jnp.float32)
+            for i, k in enumerate(direct):
+                cut = slice(i * block_rows, (i + 1) * block_rows)
+                far_src[i, 0] = cot_far[cut].astype(far_src.dtype)
+                far_src[i, 1] = inp_far[cut].astype(far_src.dtype)
         rows[0, 0] = cot_out[:block_rows].astype(rows.dtype)
         rows[1, 0] = inp_out[:block_rows].astype(rows.dtype)
 
@@ -280,6 +290,11 @@
                     remote(piece, piece, send_sem.at[2], recv_xy.at[k - 2, m - 1], me, peer[m])
                 )
 
+    def send_direct():
+        for i, k in enumerate(direct):
+            piece = rows.at[:, k, :, columns(peer[3])]
+            start(remote(far_src.at[i], piece, send_sem.at[12], recv_far.at[0, k - 2], at[k], q))
+
     def relay(g):
         for k in range(*groups[g]):
             if k < 2:
@@ -289,7 +304,7 @@
                     continue
                 piece = rows.at[:, k, :, columns(peer[m])]
                 remote(piece, piece, send_sem.at[2], recv_xy.at[k - 2, m - 1], me, q).wait_recv()
-                if square:
+                if square and k not in direct:
                     a = m - 1
                     half = rows.at[a, k, :, columns(peer[m])]
                     start(
@@ -300,7 +315,10 @@
         for k in range(*groups[g]):
             if k == 1:
                 remote(pair_src, rows.at[:, 1], send_sem.at[1], recv_z.at[1], me, q).wait_recv()
-            if k >= 2 and square:
+            if k in direct:
+                piece = rows.at[:, k, :, columns(peer[3])]
+                remote(piece, piece, send_sem.at[12], recv_far.at[0, k - 2], me, q).wait_recv()
+            elif k >= 2 and square:
                 for a in range(2):
                     piece = rows.at[a, k, :, columns(peer[3])]
                     remote(piece, piece, send_sem.at[3], recv_far.at[a, k - 2], me, q).wait_recv()
@@ -457,6 +475,7 @@
         land(1)
     with jax.named_scope("hop#g=0"):
         hop(0)
+    send_direct()
     with jax.named_scope("relay#g=1"):
         relay(1)
     with jax.named_scope("land#g=2"):
@@ -468,32 +487,32 @@
     with jax.named_scope("relay#g=2"):
         relay(2)
     flush()
+    with jax.named_scope("settle#g=2"):
+        settle(2)
     with jax.named_scope("land#g=3"):
         land(3)
-    with jax.named_scope("settle#g=2"):
-        settle(2)
+    with jax.named_scope("hop#g=1"):
+        hop(1)
     with jax.named_scope("forward#g=2"):
         forward(2)
     flush()
+    with jax.named_scope("give#g=0"):
+        give_back(0)
     with jax.named_scope("relay#g=3"):
         relay(3)
-    with jax.named_scope("hop#g=1"):
-        hop(1)
-    with jax.named_scope("give#g=0"):
-        give_back(0)
-    with jax.named_scope("hop#g=2"):
-        hop(2)
     with jax.named_scope("settle#g=3"):
         settle(3)
     with jax.named_scope("forward#g=3"):
         forward(3)
+    with jax.named_scope("hop#g=2"):
+        hop(2)
     flush()
     with jax.named_scope("give#g=1"):
         give_back(1)
+    with jax.named_scope("grad_down"):
+        down_grads()
     with jax.named_scope("give#g=2"):
         give_back(2)
-    with jax.named_scope("grad_down"):
-        down_grads()
     with jax.named_scope("hop#g=3"):
         hop(3)
     with jax.named_scope("grad_gate"):
@@ -659,7 +678,7 @@
             rows.at[:, others, :, pl.ds(0, width)],
             pair_src,
             rows.at[:, others, :, pl.ds(0, crossing * width)],
-            rows.at[:, others, :, pl.ds(0, width)] if square else None,
+            rows.at[:, pl.ds(0, sp_count - 2 - len(direct)), :, pl.ds(0, width)] if square else None,
             state_all.at[pl.ds(0, sp_count - 1)],
             part.at[pl.ds(0, 2)] if square else part,
             part.at[2] if square else None,
@@ -668,6 +687,7 @@
             pair_in,
             proj_out.at[pl.ds(0, sp_count // 2 - 1)],
             query_all.at[pl.ds(0, sp_count - 1)],
+            rows.at[:, pl.ds(0, len(direct)), :, pl.ds(0, width)] if square else None,
         ]
         for i, piece in enumerate(sent):
             if piece is not None:
@@ -752,6 +772,7 @@
             vmem((all_rows, tokens), jnp.bfloat16),
             vmem((ids.shape[0] * tokens, model_width), kind),
             vmem((sp_count, 2, block_rows, width), kind),
+            vmem((quarter, 2, block_rows, width), kind),
             vmem((2, block_rows, model_width), kind),
             vmem((2, sp_count, block_rows, model_width), kind),
             vmem((2, state_rows, value_size), full),
@@ -777,7 +798,7 @@
             vmem((sp_count, block_rows, width), kind),
             vmem((sp_count, block_rows, width), kind),
             dma((14,)),
-            dma((12,)),
+            dma((13,)),
             dma((sp_count,)),
             dma((sp_count - 2, crossing)),
             dma((2, sp_count - 2)),

time: 73.7 us -> 72.9 us (0.989)
  Pallas kernels: 72.9 us -> 72.1 us
    pallas_call x1, Pallas kernels: 70.2 us -> 69.4 us  [experts(): pl.pallas_call(functools.partial(experts_kernel, sp_count, tp_count, orde...]
where the time goes in v4:
time: 72.9 us; the launch traced here: 72.8 us
  Pallas kernels  72.1 us (99%)
    pallas_call x1, Pallas kernels, experts(): pl.pallas_call(functools.partial(experts_kernel, sp_count, tp_count, orde...  69.4 us
    pallas_call x1, Pallas kernels, store(): pl.pallas_call(store_kernel, out_shape=tuple((jax.ShapeDtypeStruct(a.shap...  2.77 us

profile of v4, /device:TPU:0, one launch (start us, length us, event | category | flops | bytes accessed | tf_op | source)
XLA Modules:
  0.0 72.8 jit_solution(17457107972986208659)
XLA Ops:
  0.6 69.4 %shard_map.189 = (bf16[2048,512]{1,0:T(8,128)(2,1)S(1)}, bf16[2048,512]{1,0:T(8,128)(2,1)S(1)}, bf16[512,2048]{1,0:T(8,128)(2,1)S(1)}, f32[256,128]{1,0:T(8,128)...) custom-call(s32[2,128]{1,0:T(2,128)} %bitcast.6, f32[1,128]{1,0:T(1,128)} %bitcast.8, ...), custom_call_target="tpu_custom_call" | custom-call | tf_op jit(solution)/shard_map/pallas_call | solution.py:743
  70.0 2.8 %shard_map.190 = (bf16[2048,512]{1,0:T(8,128)(2,1)}, bf16[2048,512]{1,0:T(8,128)(2,1)}, bf16[512,2048]{1,0:T(8,128)(2,1)}, f32[256,128]{1,0:T(8,128)}, f32[64,12...) custom-call(bf16[2048,512]{1,0:T(8,128)(2,1)S(1)} %get-tuple-element.21.refs_0_, ...), custom_call_target="tpu_custom_call" | custom-call | tf_op jit(solution)/shard_map/pallas_call | solution.py:709

commit v5 on v4

--- a/solution.py
+++ b/solution.py
@@ -517,11 +517,11 @@
         hop(3)
     with jax.named_scope("grad_gate"):
         input_grads(gate_grad, grad_gate)
-    with jax.named_scope("give#g=3"):
-        give_back(3)
     with jax.named_scope("carry"):
         score_stage()
         carry_stage()
+    with jax.named_scope("give#g=3"):
+        give_back(3)
     with jax.named_scope("back"):
         piece = returned.at[pl.ds(0, sp_count - 1)]
         remote(piece, piece, send_sem.at[7], recv_all.at[1], me, q).wait_recv()

time: 72.9 us -> 72.9 us (level)
  no operation moved by 1% of the time
where the time goes in v5:
time: 72.9 us; the launch traced here: 72.8 us
  Pallas kernels  72.1 us (99%)
    pallas_call x1, Pallas kernels, experts(): pl.pallas_call(functools.partial(experts_kernel, sp_count, tp_count, orde...  69.4 us
    pallas_call x1, Pallas kernels, store(): pl.pallas_call(store_kernel, out_shape=tuple((jax.ShapeDtypeStruct(a.shap...  2.77 us

profile of v5, /device:TPU:0, one launch (start us, length us, event | category | flops | bytes accessed | tf_op | source)
XLA Modules:
  0.0 72.8 jit_solution(697663433795370516)
XLA Ops:
  0.6 69.4 %shard_map.189 = (bf16[2048,512]{1,0:T(8,128)(2,1)S(1)}, bf16[2048,512]{1,0:T(8,128)(2,1)S(1)}, bf16[512,2048]{1,0:T(8,128)(2,1)S(1)}, f32[256,128]{1,0:T(8,128)...) custom-call(s32[2,128]{1,0:T(2,128)} %bitcast.6, f32[1,128]{1,0:T(1,128)} %bitcast.8, ...), custom_call_target="tpu_custom_call" | custom-call | tf_op jit(solution)/shard_map/pallas_call | solution.py:743
  70.0 2.8 %shard_map.190 = (bf16[2048,512]{1,0:T(8,128)(2,1)}, bf16[2048,512]{1,0:T(8,128)(2,1)}, bf16[512,2048]{1,0:T(8,128)(2,1)}, f32[256,128]{1,0:T(8,128)}, f32[64,12...) custom-call(bf16[2048,512]{1,0:T(8,128)(2,1)S(1)} %get-tuple-element.21.refs_0_, ...), custom_call_target="tpu_custom_call" | custom-call | tf_op jit(solution)/shard_map/pallas_call | solution.py:709
